TPU v7x, 32 devices: a whole 2x2x4 slice. The times are simulated.
32 devices in a mesh: fs: 8 (over z, y), tp: 4 (over x, core).
Axes of the slice: x: 2, y: 2, z: 4, core: 2. Of those that a mesh axis runs over, the one named last changes fastest.
Arguments:
- tokens: bfloat16 [16, 384, 2048], P('fs', None, 'tp'), may hold values from -34 to 34
- mix_gain: float32 [2048], replicated, may hold values from 0.1 to 1.9
- w_bgate: float32 [2048, 2048], P('fs', 'tp'), may hold values from -0.125 to 0.125
- w_cgate: float32 [2048, 2048], P('fs', 'tp'), may hold values from -0.125 to 0.125
- w_value: float32 [2048, 2048], P('fs', 'tp'), may hold values from -0.125 to 0.125
- in_scale: float32 [3, 2048], P(None, 'tp'), may hold values from 0.5 to 2
- mix_taps: float32 [3, 2048], P(None, 'tp'), may hold values from -3.5 to 3.5
- w_mixout: float32 [2048, 2048], P('tp', 'fs'), may hold values from -0.125 to 0.125
- mixout_scale: float32 [1, 2048], P(None, 'fs'), may hold values from 0.5 to 2
- ffn_gain: float32 [2048], replicated, may hold values from 0.1 to 1.9
- w_upgate: float32 [2048, 5632], P('fs', 'tp'), may hold values from -0.125 to 0.125
- w_upval: float32 [2048, 5632], P('fs', 'tp'), may hold values from -0.125 to 0.125
- up_scale: float32 [2, 5632], P(None, 'tp'), may hold values from 0.5 to 2
- ffn_taps: float32 [2, 3, 5632], P(None, None, 'tp'), may hold values from -3.5 to 3.5
- w_down: float32 [5632, 2048], P('tp', 'fs'), may hold values from -0.078125 to 0.078125
- down_scale: float32 [1, 2048], P(None, 'fs'), may hold values from 0.5 to 2
Outputs:
- layer_out: bfloat16 [16, 384, 2048], P('fs', None, 'tp')
All inputs are finite; a program needn't handle non-finite values.
Results may differ from a plain program's by a relative error of at most 0.015.
Values may be sent and summed in bfloat16 or wider, within the bound.
No kernel may reach another device: no remote copies, remote signals or barrier semaphores. Data moves between devices by JAX's collectives and lax.ppermute only.
A program may use at most 64 MiB of HBM per device.

v0:
```python
import jax
import jax.numpy as jnp
from jax import lax
from jax.experimental import pallas as pl
from jax.experimental.pallas import tpu as pltpu
from jax.sharding import Mesh, PartitionSpec as P

EPS = 1e-06
LANES = 128
PAIR = [(0, 1), (1, 0)]
PLANE = ("y", "x", "c")


def split_axes(mesh):
    fs, tp = mesh.shape["fs"], mesh.shape["tp"]
    cores = 2 if tp % 2 == 0 else 1
    nx = tp // cores
    ny = nx if fs % nx == 0 else 1
    return fs // ny, ny, nx, cores


def pick(pieces, index):
    out = pieces[0]
    for i in range(1, len(pieces)):
        out = jnp.where(index == i, pieces[i], out)
    return out


def pieces_of(values, axis, count):
    size = values.shape[axis] // count
    return [lax.slice_in_dim(values, i * size, (i + 1) * size, axis=axis) for i in range(count)]


def ring(axis, shift):
    n = lax.axis_size(axis)
    return [(i, (i + shift) % n) for i in range(n)]


def exchange(pieces, axis):
    n = lax.axis_size(axis)
    own = lax.axis_index(axis)
    out = [pick(pieces, own)]
    for s in range(1, n):
        out.append(lax.ppermute(pick(pieces, (own + s) % n), axis, ring(axis, s)))
    return out


def line_hop(chunks, step):
    n = lax.axis_size("z")
    up, down = chunks
    return (
        lax.ppermute(up, "z", [(i, i + 1) for i in range(step - 1, n - 1)]),
        lax.ppermute(down, "z", [(i, i - 1) for i in range(1, n - step + 1)]),
    )


def line_order(hops):
    n = lax.axis_size("z")
    own = lax.axis_index("z")
    return [hops[0][0]] + [jnp.where(own >= s, hops[s][0], hops[n - s][1]) for s in range(1, n)]


def line_gather(chunk):
    hops = [(chunk, chunk)]
    for step in range(1, lax.axis_size("z")):
        hops.append(line_hop(hops[-1], step))
    return line_order(hops)


def gather_weight(parts):
    nz, ny = lax.axis_size("z"), lax.axis_size("y")
    z, y = lax.axis_index("z"), lax.axis_index("y")
    shape = parts[0].shape
    out = jnp.zeros((nz, ny) + shape, parts[0].dtype)
    zero = jnp.zeros((), z.dtype)
    for t in range(ny):
        for s, chunk in enumerate(line_gather(parts[t])):
            at = ((z - s) % nz, (y - t) % ny) + (zero,) * len(shape)
            out = lax.dynamic_update_slice(out, chunk[None, None], at)
    return out


def causal_taps(values, taps):
    length = values.shape[1]
    kernel = taps.shape[0]
    padded = jnp.pad(values, ((0, 0), (kernel - 1, 0), (0, 0)))
    result = jnp.zeros(values.shape, jnp.float32)
    for offset in range(kernel):
        result = result + padded[:, offset : offset + length] * taps[offset]
    return result


def plane_rows(shard):
    wide = lax.all_gather(shard, ("x", "c"), axis=2, tiled=True)
    return lax.all_gather(wide, "y", axis=0, tiled=True)


def normed_rows(values, gain):
    floats = values.astype(jnp.float32)
    factor = lax.rsqrt(jnp.mean(floats * floats, axis=-1, keepdims=True) + EPS)
    result = (floats * factor * gain).astype(jnp.bfloat16)
    return result.reshape(-1, result.shape[-1])


def dot_rows(inputs, matrix):
    return jnp.dot(inputs, matrix, preferred_element_type=jnp.float32)


def reduce_along(values, axis, dim):
    got = exchange(pieces_of(values, dim, lax.axis_size(axis)), axis)
    total = got[0].astype(jnp.float32)
    for part in got[1:]:
        total = total + part.astype(jnp.float32)
    return total


def column_blocks(acts, blocks, scales):
    flat = blocks.reshape((-1,) + blocks.shape[2:])
    outs = [dot_rows(acts, flat[g]) for g in range(flat.shape[0])]
    return (jnp.concatenate(outs, axis=1) * scales).astype(jnp.bfloat16)


def scatter_rows(terms):
    part = terms
    part = reduce_along(part, "c", 2).astype(jnp.bfloat16)
    part = reduce_along(part, "x", 1).astype(jnp.bfloat16)
    part = part.reshape(part.shape[0], -1)
    return reduce_along(part, "y", 0)


def on_device_plain(
    tokens,
    mix_gain,
    w_bgate,
    w_cgate,
    w_value,
    in_scale,
    mix_taps,
    w_mixout,
    mixout_scale,
    ffn_gain,
    w_upgate,
    w_upval,
    up_scale,
    ffn_taps,
    w_down,
    down_scale,
):
    ny, nx = lax.axis_size("y"), lax.axis_size("x")
    y = lax.axis_index("y")
    seq_count, length, own_width = tokens.shape
    row_count = seq_count * length
    seqs = seq_count * ny

    def mine(values, axis):
        return pick(pieces_of(values, axis, ny), y)

    def exchanged(matrix, axis):
        return exchange([p.astype(jnp.bfloat16) for p in pieces_of(matrix, axis, ny)], "y")

    mix_scales, down_scales = (
        lax.all_gather(mixout_scale, ("z", "y"), axis=1, tiled=True),
        lax.all_gather(down_scale, ("z", "y"), axis=1, tiled=True),
    )

    def gather_columns(*matrices):
        parts = [exchanged(m, 1) for m in matrices]
        return gather_weight([jnp.concatenate(p, axis=1) for p in zip(*parts)])

    win = gather_columns(w_bgate, w_cgate, w_value)
    wmix = gather_weight(exchanged(w_mixout, 0))
    wgate = gather_columns(w_upgate)
    wval = gather_columns(w_upval)
    wdown = gather_weight(exchanged(w_down, 0))

    normed = normed_rows(plane_rows(tokens), mix_gain)
    scales = mine(in_scale, 1)
    mixed = dot_rows(normed, win.reshape(-1, win.shape[-1]))
    bgate, cgate, value = pieces_of(mixed, 1, 3)
    bgate = bgate * scales[0]
    inner = cgate * scales[1] * (value * scales[2])
    width = inner.shape[1]
    convolved = causal_taps(inner.reshape(seqs, length, width), mine(mix_taps, 1))
    gated = (bgate.reshape(seqs, length, width) * convolved).astype(jnp.bfloat16).reshape(-1, width)
    terms = column_blocks(gated, wmix, mix_scales)
    mix = scatter_rows(terms.reshape(terms.shape[0], nx, -1))
    resid = (tokens.reshape(row_count, own_width).astype(jnp.float32) + mix).astype(jnp.bfloat16)

    normed_ffn = normed_rows(plane_rows(resid.reshape(seq_count, length, own_width)), ffn_gain)
    scales = mine(up_scale, 1)
    taps = mine(ffn_taps, 2)
    ff = wgate.shape[-1]
    gate_pre = dot_rows(normed_ffn, wgate.reshape(-1, ff)) * scales[0]
    val_pre = dot_rows(normed_ffn, wval.reshape(-1, ff)) * scales[1]
    gate_conv = causal_taps(gate_pre.reshape(seqs, length, ff), taps[0])
    val_conv = causal_taps(val_pre.reshape(seqs, length, ff), taps[1])
    active = (jax.nn.silu(gate_conv) * val_conv).astype(jnp.bfloat16).reshape(-1, ff)
    terms = column_blocks(active, wdown, down_scales)
    ffn = scatter_rows(terms.reshape(terms.shape[0], nx, -1))
    layer_out = (resid.astype(jnp.float32) + ffn).astype(jnp.bfloat16)
    return layer_out.reshape(seq_count, length, own_width)


def split_terms(values):
    high = lax.reduce_precision(values, 8, 7)
    rest = values - high
    middle = lax.reduce_precision(rest, 8, 7)
    return [t.astype(jnp.bfloat16) for t in (high, middle, rest - middle)]


def swap(values, axis):
    return lax.ppermute(values, axis, PAIR)


def call(kernel, grid, in_specs, out_specs, out_shape, scratch, flops, order, *arrays):
    return pl.pallas_call(
        kernel,
        grid_spec=pltpu.PrefetchScalarGridSpec(
            num_scalar_prefetch=1,
            grid=grid,
            in_specs=in_specs,
            out_specs=out_specs,
            scratch_shapes=scratch,
        ),
        out_shape=out_shape,
        cost_estimate=pl.CostEstimate(flops=flops, bytes_accessed=8 << 20, transcendentals=0),
        compiler_params=pltpu.CompilerParams(
            dimension_semantics=("arbitrary",), vmem_limit_bytes=30 << 20
        ),
    )(order, *arrays)


def whole(array):
    rank = array.ndim
    return pl.BlockSpec(array.shape, lambda i, order: (0,) * rank)


def shifted_rows(values, shift):
    row = lax.broadcasted_iota(jnp.int32, values.shape, 0)
    return jnp.where(row >= shift, pltpu.roll(values, shift, axis=0), 0.0)


def conv_rows(values, taps):
    last = taps.shape[0] - 1
    total = values * taps[last : last + 1]
    for k in range(last):
        total = total + shifted_rows(values, last - k) * taps[k : k + 1]
    return total


def norm_into(order, blocks, gain, rows):
    squares = 0.0
    for block in blocks:
        floats = block[...].astype(jnp.float32)
        squares = squares + jnp.sum(floats * floats, axis=-1, keepdims=True)
    width = blocks[0].shape[-1]
    factor = lax.rsqrt(squares / (width * len(blocks)) + EPS)
    for j, block in enumerate(blocks):
        normed = block[...].astype(jnp.float32) * factor * gain[order[j]]
        at = pl.multiple_of(order[j] * width, LANES)
        rows[:, pl.ds(at, width)] = normed.astype(jnp.bfloat16)


def scaled_terms(acts, matrix, scale):
    terms = scale.astype(jnp.float32)
    total = terms[0:1] + terms[1:2] + terms[2:3]
    part = jnp.dot(acts, matrix, preferred_element_type=jnp.float32)
    return (part * total).astype(jnp.bfloat16)


def mixer_kernel(order, b0, b1, b2, b3, gain, weights, scales, taps, keep, send, rows):
    norm_into(order, (b0, b1, b2, b3), gain, rows)
    width = weights.shape[-1]
    unit = weights.shape[0] * weights.shape[1]
    k = rows.shape[1] // unit

    def project(m):
        matrix = weights[:, :, m * k : (m + 1) * k, :].reshape(unit * k, width)
        result = jnp.dot(rows[...], matrix, preferred_element_type=jnp.float32)
        return result * scales[m : m + 1]

    inner = project(1) * project(2)
    gated = (project(0) * conv_rows(inner, taps[...])).astype(jnp.bfloat16)
    low = 3 * k
    for j in range(4):
        for h in range(2):
            matrix, scale = weights[order[j], h, low : low + width, :], weights[order[j], h, low + width :, :]
            (keep, send)[j // 2][j % 2, h] = scaled_terms(gated, matrix, scale)


def up_kernel(order, b0, b1, b2, b3, gain, weights, scales, taps, active, rows):
    norm_into(order, (b0, b1, b2, b3), gain, rows)
    both = weights.shape[-1]
    hidden = both // 2
    matrix = weights[...].reshape(rows.shape[1], both)
    pre = jnp.dot(rows[...], matrix, preferred_element_type=jnp.float32) * scales[...]
    conv = conv_rows(pre, taps[...])
    full = hidden // LANES * LANES
    gate, value = conv[:, :full], conv[:, both - full :]
    active[:, :full] = (gate / (1.0 + jnp.exp(-gate)) * value).astype(jnp.bfloat16)
    if full < hidden:
        mixed = conv[:, full : full + LANES]
        other = pltpu.roll(mixed, LANES // 2, axis=1)
        part = mixed / (1.0 + jnp.exp(-mixed)) * other
        active[:, full:] = part[:, : hidden - full].astype(jnp.bfloat16)


def down_kernel(order, active, early, late, keep, send):
    acts = active[...]
    hidden = acts.shape[1]
    for j in range(4):
        for i, weights in enumerate((late, early)):
            matrix, scale = weights[order[j], :hidden, :], weights[order[j], hidden:, :]
            (keep, send)[j // 2][j % 2, order[4 + i]] = scaled_terms(acts, matrix, scale)


def term_shapes(seqs, length, width):
    lead = (2, 2)
    shape = jax.ShapeDtypeStruct(lead + (seqs * length, width), jnp.bfloat16)
    spec = pl.BlockSpec(lead + (length, width), lambda i, order: (0, 0, i, 0))
    return (shape, shape), (spec, spec)


def plane_blocks(own):
    half = own.shape[1] // 2
    across, beside = swap(own, "x"), swap(own, "y")
    twin = swap(own, "c")
    left, right = swap(beside[:, :half], "x"), swap(across[:, half:], "y")
    corner = jnp.concatenate([left, right], axis=1)
    mine = (own, across, twin, swap(across, "c"))
    theirs = (beside, corner, swap(beside, "c"), swap(corner, "c"))
    return mine, theirs


def over_cores(terms):
    keep, send = terms
    got = swap(send, "c")
    return keep.astype(jnp.float32) + got.astype(jnp.float32)


def moved(values, axis):
    return swap(values.astype(jnp.bfloat16), axis).astype(jnp.float32)


def plane_sums(mine, theirs):
    far = over_cores(theirs)
    near = over_cores(mine)
    left_far = far[0, 0] + moved(far[1, 0], "x")
    right = near[:, 1] + moved(far[:, 1], "y")
    left_near = near[0, 0] + moved(near[1, 0], "x")
    left, right = left_near + moved(left_far, "y"), right[0] + moved(right[1], "x")
    return jnp.concatenate([left, right], axis=1)


def on_device(
    tokens,
    mix_gain,
    w_bgate,
    w_cgate,
    w_value,
    in_scale,
    mix_taps,
    w_mixout,
    mixout_scale,
    ffn_gain,
    w_upgate,
    w_upval,
    up_scale,
    ffn_taps,
    w_down,
    down_scale,
):
    y, x, c = (lax.axis_index(a) for a in PLANE)
    seqs, length, own_width = tokens.shape
    row_count = seqs * length
    blocks = 4

    def exchanged(lower, upper):
        keep, send = pick([lower, upper], y), pick([upper, lower], y)
        got = swap(send, "y")
        return jnp.stack([pick([keep, got], y), pick([got, keep], y)])

    def halves(matrix, axis):
        return pieces_of(matrix, axis, 2)

    def packed(gate, value):
        full = gate.shape[-1] // LANES * LANES
        return jnp.concatenate([gate, value[..., full:], value[..., :full]], axis=-1)

    def rounded(matrix):
        return matrix.astype(jnp.bfloat16)

    def scale_rows(scale):
        spare = jnp.zeros((13, scale.shape[1]), jnp.bfloat16)
        return jnp.concatenate(split_terms(scale) + [spare])

    z = lax.axis_index("z")
    own = tokens.reshape(row_count, own_width)

    ins = [halves(rounded(m), 1) for m in (w_bgate, w_cgate, w_value)]
    outs = halves(rounded(w_mixout), 0)
    mix_rows, down_rows = scale_rows(mixout_scale), scale_rows(down_scale)
    downs = [jnp.concatenate([d, down_rows]) for d in halves(rounded(w_down), 0)]
    early = pick(downs, y)
    hops = [(early, early)]
    hops.append(line_hop(hops[-1], 1))
    mixer_own = exchanged(*(jnp.concatenate([m[i] for m in ins] + [outs[i], mix_rows]) for i in range(2)))
    mixer_own, hops = lax.optimization_barrier((mixer_own, hops))
    mixer_w = lax.all_gather(mixer_own, "z")
    hops.append(line_hop(hops[-1], 2))
    hops.append(line_hop(hops[-1], 3))
    early_w = jnp.stack(line_order(hops))
    ups = [
        packed(g, v) for g, v in zip(halves(rounded(w_upgate), 1), halves(rounded(w_upval), 1))
    ]
    up_own = exchanged(*ups)
    up_w = lax.all_gather(up_own, "z")
    late = swap(pick(downs[::-1], y), "y")
    late_hops = [(late, late)]
    for step in (1, 2, 3):
        late_hops.append(line_hop(late_hops[-1], step))
    late_w = jnp.stack(line_order(late_hops))

    places = [jx * 2 + jc for jc in (c, 1 - c) for jx in (x, 1 - x)]

    def table(*entries):
        return jnp.stack(entries).astype(jnp.int32)

    order = table(*places)
    down_order = table(*((z - t) % blocks for t in places), 1 - y, y)

    def mine(values, axis):
        return pick(halves(values, axis), y)

    def block_specs(width):
        return [pl.BlockSpec((length, width), lambda i, order: (i, 0))] * blocks

    features = own_width * blocks
    rows_scratch = [pltpu.VMEM((length, features), jnp.bfloat16)]

    def mixer(group):
        width = mixer_w.shape[-1]
        small = (mix_gain.reshape(blocks, 1, own_width), mixer_w, mine(in_scale, 1), mine(mix_taps, 1))
        shapes, specs = term_shapes(seqs, length, width)
        flops = 2 * row_count * features * width * 4
        return call(
            mixer_kernel, (seqs,), block_specs(own_width) + [whole(a) for a in small], specs, shapes,
            rows_scratch, flops, order, *group, *small,
        )

    def up(group):
        scale = packed(*(mine(up_scale, 1)[i : i + 1] for i in range(2)))
        taps = packed(*(mine(ffn_taps, 2)[i] for i in range(2)))
        small = (ffn_gain.reshape(blocks, 1, own_width), up_w, scale, taps)
        hidden = up_w.shape[-1] // 2
        flops = 2 * row_count * features * 2 * hidden
        return call(
            up_kernel, (seqs,), block_specs(own_width) + [whole(a) for a in small],
            pl.BlockSpec((length, hidden), lambda i, order: (i, 0)),
            jax.ShapeDtypeStruct((row_count, hidden), jnp.bfloat16),
            rows_scratch, flops, order, *group, *small,
        )

    def down(active):
        hidden = active.shape[1]
        shapes, specs = term_shapes(seqs, length, early_w.shape[-1])
        flops = 2 * row_count * features * hidden
        return call(
            down_kernel, (seqs,),
            [pl.BlockSpec((length, hidden), lambda i, order: (i, 0)), whole(early_w), whole(late_w)],
            specs, shapes, [], flops, down_order, active, early_w, late_w,
        )

    def added(base, sums):
        return (base.astype(jnp.float32) + sums).astype(jnp.bfloat16)

    near, far = plane_blocks(own)
    terms_far = mixer(far)
    resid = added(own, plane_sums(mixer(near), terms_far))
    near, far = plane_blocks(resid)
    active_near, active_far = up(near), up(far)
    terms_far = down(active_far)
    layer_out = added(resid, plane_sums(down(active_near), terms_far))
    return layer_out.reshape(seqs, length, own_width)


def fits(tokens, w_bgate, w_mixout, w_upgate, w_down):
    ny, nx, nc, nz = (lax.axis_size(a) for a in PLANE + ("z",))
    return (
        (ny, nx, nc) == (2, 2, 2)
        and nz * ny * w_bgate.shape[0] == nx * nc * tokens.shape[2]
        and nz == nx * nc == 4
        and w_bgate.shape[0] == w_bgate.shape[1] // ny == w_mixout.shape[0] // ny == w_mixout.shape[1]
        and w_down.shape[1] == w_mixout.shape[1]
        and w_mixout.shape[1] % (2 * LANES) == 0
        and tokens.shape[1] % 16 == 0
        and w_upgate.shape[1] // ny % (LANES // 2) == 0
        and w_down.shape[0] // ny % 16 == 0
    )


def dispatch(*args):
    if not fits(args[0], args[2], args[7], args[10], args[14]):
        return on_device_plain(*args)
    return on_device(*args)


def solution(mesh):
    fine = Mesh(mesh.devices.reshape(split_axes(mesh)), ("z",) + PLANE)
    fs, tp = ("z", "y"), ("x", "c")
    in_specs = (
        P(fs, None, tp),
        P(),
        P(fs, tp),
        P(fs, tp),
        P(fs, tp),
        P(None, tp),
        P(None, tp),
        P(tp, fs),
        P(None, fs),
        P(),
        P(fs, tp),
        P(fs, tp),
        P(None, tp),
        P(None, None, tp),
        P(tp, fs),
        P(None, fs),
    )
    out_specs = P(fs, None, tp)
    return jax.shard_map(
        dispatch, mesh=fine, in_specs=in_specs, out_specs=out_specs, check_vma=False
    )
```

profile of v0, /device:TPU:0, one launch (start us, length us, event | category | flops | bytes accessed | tf_op | source)
XLA Modules:
  0.0 327.2 jit_solution(14398814893945426338)
XLA Ops:
  6.5 1.2 convert_element_type.152
  7.7 1.1 convert_element_type.151
  9.5 3.1 collective-permute-start.3
  14.4 4.2 %collective-permute-start.4 = (bf16[720,256]{1,0:T(8,128)(2,1)S(1)}, bf16[720,256]{1,0:T(8,128)(2,1)}, u32[]{:S(2)}, u32[]{:S(2)}) collective-permute-start(bf16[720,256]{1,0:T(8,128)(2,1)S(1)} %get-tuple-element.22), channel_id=1, source_target_pairs={{0,8},{8,16},{16,24},{1,9},{9,17},{17,25},{2,10},{10,18},{18,26},{... | collective-permute-start | bytes 1105928 | tf_op jit(solution)/shard_map/ppermute | solution.py:52
  18.7 1.3 collective-permute-start.5
  20.0 4.8 %collective-permute-done.3 = bf16[1040,256]{1,0:T(8,128)(2,1)} collective-permute-done((bf16[1040,256]{1,0:T(8,128)(2,1)S(1)}, bf16[1040,256]{1,0:T(8,128)(2,1)}, u32[]{:S(2)}, u32[]{:S(2)}) %collective-permute-start.3) | collective-permute-done | bytes 532512 | tf_op jit(solution)/shard_map/ppermute | solution.py:212
  24.7 1.1 select_bitcast_fusion.3
  25.9 1.1 pad_maximum_fusion.3
  27.0 3.4 %collective-permute-done.5 = bf16[720,256]{1,0:T(8,128)(2,1)} collective-permute-done((bf16[720,256]{1,0:T(8,128)(2,1)S(1)}, bf16[720,256]{1,0:T(8,128)(2,1)}, u32[]{:S(2)}, u32[]{:S(2)}) %collective-permute-start.5) | collective-permute-done | bytes 368672 | tf_op jit(solution)/shard_map/ppermute | solution.py:53
  30.5 1.4 collective-permute-start.8
  33.5 1.1 concatenate.66
  35.5 1.2 collective-permute-start.21
  36.7 1.5 collective-permute-start
  38.2 12.8 %collective-permute-done.8.b0 = bf16[768,512]{1,0:T(8,128)(2,1)S(1)} collective-permute-done((bf16[768,512]{1,0:T(8,128)(2,1)S(1)}, bf16[768,512]{1,0:T(8,128)(2,1)S(1)}, u32[]{:S(2)}, u32[]{:S(2)}) %collective-permute-start.8) | collective-permute-done | bytes 786464 | tf_op jit(solution)/shard_map/ppermute | solution.py:212
  51.8 1.5 collective-permute-start.9
  53.3 10.6 %collective-permute-done.21 = bf16[256,1408]{1,0:T(8,128)(2,1)S(1)} collective-permute-done((bf16[256,1408]{1,0:T(8,128)(2,1)S(1)}, bf16[256,1408]{1,0:T(8,128)(2,1)S(1)}, u32[]{:S(2)}, u32[]{:S(2)}) %collective-permute-start.21) | collective-permute-done | bytes 720928 | tf_op jit(solution)/shard_map/ppermute | solution.py:212
  64.8 2.7 collective-permute-start.10
  67.5 1.3 pad_maximum_fusion.2
  69.0 6.1 %collective-permute-done.10 = bf16[768,256]{1,0:T(8,128)(2,1)} collective-permute-done((bf16[768,256]{1,0:T(8,128)(2,1)}, bf16[768,256]{1,0:T(8,128)(2,1)}, u32[]{:S(2)}, u32[]{:S(2)}) %collective-permute-start.10) | collective-permute-done | bytes 393248 | tf_op jit(solution)/shard_map/ppermute | solution.py:212
  78.6 33.1 %all-gather.5.cloned.1.call-done = bf16[8,1040,256]{2,1,0:T(8,128)(2,1)} async-done(((bf16[2,1040,256]{2,1,0:T(8,128)(2,1)}), bf16[8,1040,256]{2,1,0:T(8,128)(2,1)}) %all-gather.5.cloned.1.call-update) | async-done | bytes 4259856 | tf_op jit(solution)/shard_map/all_gather | solution.py:409
  111.7 2.2 copy-done.4
  113.9 9.1 %shard_map.155 = (bf16[2,2,768,256]{3,2,1,0:T(8,128)(2,1)S(1)}, bf16[2,2,768,256]{3,2,1,0:T(8,128)(2,1)S(1)}) custom-call(s32[4]{0:T(128)S(1)} %pad_add_fusion.order, bf16[768,512]{1,0:T(8,128)(2,1)S(1)} %collective-permute-done.8.b0, bf16[768,512]{1,0:T(8,128)(2,1)S(1)} %constant_dynamic-update-slice_fusion.b1, ...), custom_call_target="tpu_custom_call" | custom-call | flops 3221225472 | bytes 8388608 | tf_op jit(solution)/shard_map/pallas_call | solution.py:216
  123.2 8.8 %shard_map.154 = (bf16[2,2,768,256]{3,2,1,0:T(8,128)(2,1)S(1)}, bf16[2,2,768,256]{3,2,1,0:T(8,128)(2,1)S(1)}) custom-call(s32[4]{0:T(128)S(1)} %pad_add_fusion.order, bf16[768,512]{1,0:T(8,128)(2,1)S(1)} %bitcast.107, bf16[768,512]{1,0:T(8,128)(2,1)S(1)} %collective-permute-done.b1, bf16[768,512]{1,0:T(8,128)(2,1)} %collective-permute-done.1.b2, ...), custom_call_target="tpu_custom_call" | custom-call | flops 3221225472 | bytes 8388608 | tf_op jit(solution)/shard_map/pallas_call | solution.py:216
  132.6 1.5 collective-permute-start.26
  135.3 1.5 collective-permute-start.14
  137.8 9.5 %collective-permute-done.14 = bf16[768,256]{1,0:T(8,128)(2,1)S(1)} collective-permute-done((bf16[768,256]{1,0:T(8,128)(2,1)S(1)}, bf16[768,256]{1,0:T(8,128)(2,1)S(1)}, u32[]{:S(2)}, u32[]{:S(2)}) %collective-permute-start.14) | collective-permute-done | bytes 393248 | tf_op jit(solution)/shard_map/ppermute | solution.py:212
  147.4 1.5 collective-permute-start.15
  149.0 11.9 %collective-permute-done.16 = bf16[2,768,256]{2,1,0:T(8,128)(2,1)S(1)} collective-permute-done((bf16[2,768,256]{2,1,0:T(8,128)(2,1)S(1)}, bf16[2,768,256]{2,1,0:T(8,128)(2,1)S(1)}, u32[]{:S(2)}, u32[]{:S(2)}) %collective-permute-start.16) | collective-permute-done | bytes 786464 | tf_op jit(solution)/shard_map/ppermute | solution.py:212
  161.2 1.5 collective-permute-start.17
  162.7 1.3 collective-permute-start.27
  164.0 1.3 collective-permute-start.28
  166.0 2.4 collective-permute-done.15
  168.4 1.5 collective-permute-start.22
  171.7 1.4 collective-permute-start.18
  173.2 6.9 %collective-permute-done.27 = bf16[720,256]{1,0:T(8,128)(2,1)S(1)} collective-permute-done((bf16[720,256]{1,0:T(8,128)(2,1)S(1)}, bf16[720,256]{1,0:T(8,128)(2,1)S(1)}, u32[]{:S(2)}, u32[]{:S(2)}) %collective-permute-start.27) | collective-permute-done | bytes 368672 | tf_op jit(solution)/shard_map/ppermute | solution.py:52
  180.1 1.5 collective-permute-start.35
  181.7 12.3 %collective-permute-done.28 = bf16[720,256]{1,0:T(8,128)(2,1)S(1)} collective-permute-done((bf16[720,256]{1,0:T(8,128)(2,1)S(1)}, bf16[720,256]{1,0:T(8,128)(2,1)S(1)}, u32[]{:S(2)}, u32[]{:S(2)}) %collective-permute-start.28) | collective-permute-done | bytes 368672 | tf_op jit(solution)/shard_map/ppermute | solution.py:53
  193.9 1.4 collective-permute-start.31
  195.4 1.3 collective-permute-start.29
  197.0 16.7 %collective-permute-done.22 = bf16[720,256]{1,0:T(8,128)(2,1)S(1)} collective-permute-done((bf16[720,256]{1,0:T(8,128)(2,1)}, bf16[720,256]{1,0:T(8,128)(2,1)S(1)}, u32[]{:S(2)}, u32[]{:S(2)}) %collective-permute-start.22) | collective-permute-done | bytes 368672 | tf_op jit(solution)/shard_map/ppermute | solution.py:53
  214.5 1.3 collective-permute-start.23
  215.8 20.5 %collective-permute-done.29 = bf16[720,256]{1,0:T(8,128)(2,1)} collective-permute-done((bf16[720,256]{1,0:T(8,128)(2,1)S(1)}, bf16[720,256]{1,0:T(8,128)(2,1)}, u32[]{:S(2)}, u32[]{:S(2)}) %collective-permute-start.29) | collective-permute-done | bytes 368672 | tf_op jit(solution)/shard_map/ppermute | solution.py:53
  237.0 1.0 select_bitcast_fusion.5
  238.1 1.3 collective-permute-start.30
  240.4 1.9 collective-permute-start.36
  243.4 1.6 collective-permute-start.37
  244.9 1.0 select_bitcast_fusion.7
  246.0 3.0 collective-permute-done.23
  249.9 1.3 collective-permute-done.37
  253.0 3.1 collective-permute-done.30
  256.1 1.4 pad_maximum_fusion.1.late
  258.1 2.6 copy-done.2
  260.7 9.8 %shard_map.158.active = bf16[768,704]{1,0:T(8,128)(2,1)S(1)} custom-call(s32[4]{0:T(128)S(1)} %pad_add_fusion.order, bf16[768,512]{1,0:T(8,128)(2,1)} %collective-permute-done.35.b0, bf16[768,512]{1,0:T(8,128)(2,1)} %constant_dynamic-update-slice_fusion.2.b1, bf16[768,512]{1,0:T(8,128)(2,1)} %collective-permute-done.38.b2, ...), custom_call_target="tpu_custom_call" | custom-call | flops 4429185024 | bytes 8388608 | tf_op jit(solution)/shard_map/pallas_call | solution.py:216
  270.5 3.8 %shard_map.159 = (bf16[2,2,768,256]{3,2,1,0:T(8,128)(2,1)S(1)}, bf16[2,2,768,256]{3,2,1,0:T(8,128)(2,1)S(1)}) custom-call(s32[6]{0:T(128)S(1)} %stack.98.order, bf16[768,704]{1,0:T(8,128)(2,1)S(1)} %shard_map.158.active, bf16[4,720,256]{2,1,0:T(8,128)(2,1)S(1)} %pad_maximum_fusion.early, bf16[4,720,256]{2,1,0:T(8,128)(2,1)S(1)} %copy-done.1), custom_call_target="tpu_custom_call" | custom-call | flops 2214592512 | bytes 8388608 | tf_op jit(solution)/shard_map/pallas_call | solution.py:216
  274.4 9.7 %shard_map.156.active = bf16[768,704]{1,0:T(8,128)(2,1)S(1)} custom-call(s32[4]{0:T(128)S(1)} %pad_add_fusion.order, bf16[768,512]{1,0:T(8,128)(2,1)S(1)} %fusion.3.b0, bf16[768,512]{1,0:T(8,128)(2,1)} %collective-permute-done.18.b1, bf16[768,512]{1,0:T(8,128)(2,1)} %collective-permute-done.19.b2, bf16[768,512]{1,0:T(8,128)(2,1)} %collective-permute-done.20.b3, ...), custom_call_target="tpu_custom_call" | custom-call | flops 4429185024 | bytes 8388608 | tf_op jit(solution)/shard_map/pallas_call | solution.py:216
  284.1 3.8 %shard_map.157 = (bf16[2,2,768,256]{3,2,1,0:T(8,128)(2,1)S(1)}, bf16[2,2,768,256]{3,2,1,0:T(8,128)(2,1)S(1)}) custom-call(s32[6]{0:T(128)S(1)} %stack.98.order, bf16[768,704]{1,0:T(8,128)(2,1)S(1)} %shard_map.156.active, bf16[4,720,256]{2,1,0:T(8,128)(2,1)S(1)} %pad_maximum_fusion.early, bf16[4,720,256]{2,1,0:T(8,128)(2,1)S(1)} %copy-done.1), custom_call_target="tpu_custom_call" | custom-call | flops 2214592512 | bytes 8388608 | tf_op jit(solution)/shard_map/pallas_call | solution.py:216
  289.0 1.6 collective-permute-start.43
  290.7 1.5 collective-permute-start.41
  293.6 9.2 %collective-permute-done.41 = bf16[768,256]{1,0:T(8,128)(2,1)S(1)} collective-permute-done((bf16[768,256]{1,0:T(8,128)(2,1)S(1)}, bf16[768,256]{1,0:T(8,128)(2,1)S(1)}, u32[]{:S(2)}, u32[]{:S(2)}) %collective-permute-start.41) | collective-permute-done | bytes 393248 | tf_op jit(solution)/shard_map/ppermute | solution.py:212
  303.3 6.1 %collective-permute-done.43 = bf16[2,768,256]{2,1,0:T(8,128)(2,1)S(1)} collective-permute-done((bf16[2,768,256]{2,1,0:T(8,128)(2,1)S(1)}, bf16[2,768,256]{2,1,0:T(8,128)(2,1)S(1)}, u32[]{:S(2)}, u32[]{:S(2)}) %collective-permute-start.43) | collective-permute-done | bytes 786464 | tf_op jit(solution)/shard_map/ppermute | solution.py:212
  309.7 1.6 collective-permute-start.44
  311.3 5.7 %collective-permute-done.42 = bf16[768,256]{1,0:T(8,128)(2,1)S(1)} collective-permute-done((bf16[768,256]{1,0:T(8,128)(2,1)S(1)}, bf16[768,256]{1,0:T(8,128)(2,1)S(1)}, u32[]{:S(2)}, u32[]{:S(2)}) %collective-permute-start.42) | collective-permute-done | bytes 393248 | tf_op jit(solution)/shard_map/ppermute | solution.py:212
  317.1 2.0 collective-permute-done.44
  319.2 1.2 fusion.4
  (178 shorter events, 26.7 us)
Async XLA Ops:
  6.5 105.2 %all-gather.5.cloned.1.call-start = ((), (), s32[]{:S(2)}) async-start(), calls=%async_computation | async-start | bytes 5324800 | tf_op jit(solution)/shard_map/all_gather | solution.py:409
  9.2 3.3 %copy-start.28 = (f32[1,256]{1,0:T(1,128)S(1)}, f32[1,256]{1,0:T(1,128)}, u32[]{:S(2)}) copy-start(f32[1,256]{1,0:T(1,128)} %param.31) | copy-start | bytes 3076
  9.2 3.3 %copy-start.15 = (f32[1408,256]{1,0:T(8,128)S(1)}, f32[1408,256]{1,0:T(8,128)}, u32[]{:S(2)}) copy-start(f32[1408,256]{1,0:T(8,128)} %param.30) | copy-start | bytes 4325380
  9.5 15.3 %collective-permute-start.3 = (bf16[1040,256]{1,0:T(8,128)(2,1)S(1)}, bf16[1040,256]{1,0:T(8,128)(2,1)}, u32[]{:S(2)}, u32[]{:S(2)}) collective-permute-start(bf16[1040,256]{1,0:T(8,128)(2,1)S(1)} %broadcast_select_fusion.3), channel_id=1, source_target_pairs={{0,4},{4,0},{1,5},{5,1},{2,6},{6,2},{3,7},{7,3},{8,12},{12,8},{9,1... | collective-permute-start | bytes 1597448 | tf_op jit(solution)/shard_map/ppermute | solution.py:212
  14.4 12.6 %copy-start.13 = (bf16[720,256]{1,0:T(8,128)(2,1)}, bf16[720,256]{1,0:T(8,128)(2,1)S(1)}, u32[]{:S(2)}) copy-start(bf16[720,256]{1,0:T(8,128)(2,1)S(1)} %get-tuple-element.22) | copy-start | bytes 1105924
  14.4 12.6 %collective-permute-start.4 = (bf16[720,256]{1,0:T(8,128)(2,1)S(1)}, bf16[720,256]{1,0:T(8,128)(2,1)}, u32[]{:S(2)}, u32[]{:S(2)}) collective-permute-start(bf16[720,256]{1,0:T(8,128)(2,1)S(1)} %get-tuple-element.22), channel_id=1, source_target_pairs={{0,8},{8,16},{16,24},{1,9},{9,17},{17,25},{2,10},{10,18},{18,26},{... | collective-permute-start | bytes 1105928 | tf_op jit(solution)/shard_map/ppermute | solution.py:52
  18.7 11.8 %collective-permute-start.5 = (bf16[720,256]{1,0:T(8,128)(2,1)S(1)}, bf16[720,256]{1,0:T(8,128)(2,1)}, u32[]{:S(2)}, u32[]{:S(2)}) collective-permute-start(bf16[720,256]{1,0:T(8,128)(2,1)S(1)} %get-tuple-element.22), channel_id=1, source_target_pairs={{8,0},{16,8},{24,16},{9,1},{17,9},{25,17},{10,2},{18,10},{26,18},{... | collective-permute-start | bytes 1105928 | tf_op jit(solution)/shard_map/ppermute | solution.py:53
  25.9 4.6 %copy-start = (bf16[2,384,512]{2,1,0:T(8,128)(2,1)S(1)}, bf16[2,384,512]{2,1,0:T(8,128)(2,1)}, u32[]{:S(2)}) copy-start(bf16[2,384,512]{2,1,0:T(8,128)(2,1)} %param.16) | copy-start | bytes 2359300
  25.9 6.0 %copy-start.16 = (f32[256,1408]{1,0:T(8,128)S(1)}, f32[256,1408]{1,0:T(8,128)}, u32[]{:S(2)}) copy-start(f32[256,1408]{1,0:T(8,128)} %param.26) | copy-start | bytes 4325380
  30.4 227.6 %all-gather.7.cloned.1.call-start = ((), (), s32[]{:S(2)}) async-start(), calls=%async_computation.1 | async-start | bytes 7208960 | tf_op jit(solution)/shard_map/all_gather | solution.py:417
  30.5 20.5 %collective-permute-start.8 = (bf16[768,512]{1,0:T(8,128)(2,1)S(1)}, bf16[768,512]{1,0:T(8,128)(2,1)S(1)}, u32[]{:S(2)}, u32[]{:S(2)}) collective-permute-start(bf16[768,512]{1,0:T(8,128)(2,1)S(1)} %bitcast.104), channel_id=1, source_target_pairs={{0,4},{4,0},{1,5},{5,1},{2,6},{6,2},{3,7},{7,3},{8,12},{12,8},{9,1... | collective-permute-start | bytes 2359304 | tf_op jit(solution)/shard_map/ppermute | solution.py:212
  35.5 28.4 %collective-permute-start.21 = (bf16[256,1408]{1,0:T(8,128)(2,1)S(1)}, bf16[256,1408]{1,0:T(8,128)(2,1)S(1)}, u32[]{:S(2)}, u32[]{:S(2)}) collective-permute-start(bf16[256,1408]{1,0:T(8,128)(2,1)S(1)} %broadcast_select_fusion.1), channel_id=1, source_target_pairs={{0,4},{4,0},{1,5},{5,1},{2,6},{6,2},{3,7},{7,3},{8,12},{12,8},{9,1... | collective-permute-start | bytes 2162696 | tf_op jit(solution)/shard_map/ppermute | solution.py:212
  36.7 27.4 %collective-permute-start = (bf16[768,512]{1,0:T(8,128)(2,1)S(1)}, bf16[768,512]{1,0:T(8,128)(2,1)S(1)}, u32[]{:S(2)}, u32[]{:S(2)}) collective-permute-start(bf16[768,512]{1,0:T(8,128)(2,1)S(1)} %bitcast.105), channel_id=1, source_target_pairs={{0,2},{2,0},{1,3},{3,1},{4,6},{6,4},{5,7},{7,5},{8,10},{10,8},{9,1... | collective-permute-start | bytes 2359304 | tf_op jit(solution)/shard_map/ppermute | solution.py:212
  51.8 17.2 %collective-permute-start.9 = (bf16[768,256]{1,0:T(8,128)(2,1)}, bf16[768,256]{1,0:T(8,128)(2,1)S(1)}, u32[]{:S(2)}, u32[]{:S(2)}) collective-permute-start(bf16[768,256]{1,0:T(8,128)(2,1)} %slice.257), channel_id=1, source_target_pairs={{0,2},{2,0},{1,3},{3,1},{4,6},{6,4},{5,7},{7,5},{8,10},{10,8},{9,1... | collective-permute-start | bytes 1179656 | tf_op jit(solution)/shard_map/ppermute | solution.py:212
  64.8 10.2 %collective-permute-start.10 = (bf16[768,256]{1,0:T(8,128)(2,1)}, bf16[768,256]{1,0:T(8,128)(2,1)}, u32[]{:S(2)}, u32[]{:S(2)}) collective-permute-start(bf16[768,256]{1,0:T(8,128)(2,1)} %slice.258), channel_id=1, source_target_pairs={{0,4},{4,0},{1,5},{5,1},{2,6},{6,2},{3,7},{7,3},{8,12},{12,8},{9,1... | collective-permute-start | bytes 1179656 | tf_op jit(solution)/shard_map/ppermute | solution.py:212
  68.8 42.9 %copy-start.6 = (f32[2048]{0:T(1024)S(1)}, f32[2048]{0:T(1024)}, u32[]{:S(2)}) copy-start(f32[2048]{0:T(1024)} %param.17) | copy-start | bytes 24580
  68.9 8.7 %collective-permute-start.11 = (bf16[768,512]{1,0:T(8,128)(2,1)S(1)}, bf16[768,512]{1,0:T(8,128)(2,1)}, u32[]{:S(2)}, u32[]{:S(2)}) collective-permute-start(bf16[768,512]{1,0:T(8,128)(2,1)S(1)} %collective-permute-done.8.b0), channel_id=1, source_target_pairs={{0,1},{1,0},{2,3},{3,2},{4,5},{5,4},{6,7},{7,6},{8,9},{9,8},{10,11... | collective-permute-start | bytes 2359304 | tf_op jit(solution)/shard_map/ppermute | solution.py:212
  76.1 2.5 collective-permute-start.12
  76.2 47.0 %collective-permute-start.1 = (bf16[768,512]{1,0:T(8,128)(2,1)S(1)}, bf16[768,512]{1,0:T(8,128)(2,1)}, u32[]{:S(2)}, u32[]{:S(2)}) collective-permute-start(bf16[768,512]{1,0:T(8,128)(2,1)S(1)} %bitcast.106), channel_id=1, source_target_pairs={{0,1},{1,0},{2,3},{3,2},{4,5},{5,4},{6,7},{7,6},{8,9},{9,8},{10,11... | collective-permute-start | bytes 2359304 | tf_op jit(solution)/shard_map/ppermute | solution.py:212
  77.5 45.7 %collective-permute-start.2 = (bf16[768,512]{1,0:T(8,128)(2,1)S(1)}, bf16[768,512]{1,0:T(8,128)(2,1)}, u32[]{:S(2)}, u32[]{:S(2)}) collective-permute-start(bf16[768,512]{1,0:T(8,128)(2,1)S(1)} %collective-permute-done.b1), channel_id=1, source_target_pairs={{0,1},{1,0},{2,3},{3,2},{4,5},{5,4},{6,7},{7,6},{8,9},{9,8},{10,11... | collective-permute-start | bytes 2359304 | tf_op jit(solution)/shard_map/ppermute | solution.py:212
  113.9 9.3 %copy-start.5 = (bf16[8,1040,256]{2,1,0:T(8,128)(2,1)S(1)}, bf16[8,1040,256]{2,1,0:T(8,128)(2,1)}, u32[]{:S(2)}) copy-start(bf16[8,1040,256]{2,1,0:T(8,128)(2,1)} %all-gather.5.cloned.1.call-done) | copy-start | bytes 12779524
  123.0 9.5 %copy-start.20 = (bf16[720,256]{1,0:T(8,128)(2,1)S(1)}, bf16[720,256]{1,0:T(8,128)(2,1)}, u32[]{:S(2)}) copy-start(bf16[720,256]{1,0:T(8,128)(2,1)} %get-tuple-element.35) | copy-start | bytes 1105924
  123.1 11.0 %copy-start.25 = (f32[2,3,1408]{2,0,1:T(2,128)S(1)}, f32[2,3,1408]{2,0,1:T(2,128)}, u32[]{:S(2)}) copy-start(f32[2,3,1408]{2,0,1:T(2,128)} %param.29) | copy-start | bytes 101380
  123.1 11.1 %collective-permute-start.13 = (bf16[2,2,768,256]{3,2,1,0:T(8,128)(2,1)S(1)}, bf16[2,2,768,256]{3,2,1,0:T(8,128)(2,1)S(1)}, u32[]{:S(2)}, u32[]{:S(2)}) collective-permute-start(bf16[2,2,768,256]{3,2,1,0:T(8,128)(2,1)S(1)} %get-tuple-element.21), channel_id=1, source_target_pairs={{0,1},{1,0},{2,3},{3,2},{4,5},{5,4},{6,7},{7,6},{8,9},{9,8},{10,11... | collective-permute-start | bytes 4718600 | tf_op jit(solution)/shard_map/ppermute | solution.py:212
  132.0 4.7 %collective-permute-start.6 = (bf16[2,2,768,256]{3,2,1,0:T(8,128)(2,1)S(1)}, bf16[2,2,768,256]{3,2,1,0:T(8,128)(2,1)S(1)}, u32[]{:S(2)}, u32[]{:S(2)}) collective-permute-start(bf16[2,2,768,256]{3,2,1,0:T(8,128)(2,1)S(1)} %get-tuple-element.19), channel_id=1, source_target_pairs={{0,1},{1,0},{2,3},{3,2},{4,5},{5,4},{6,7},{7,6},{8,9},{9,8},{10,11... | collective-permute-start | bytes 4718600 | tf_op jit(solution)/shard_map/ppermute | solution.py:212
  132.6 30.1 %collective-permute-start.26 = (bf16[720,256]{1,0:T(8,128)(2,1)S(1)}, bf16[720,256]{1,0:T(8,128)(2,1)S(1)}, u32[]{:S(2)}, u32[]{:S(2)}) collective-permute-start(bf16[720,256]{1,0:T(8,128)(2,1)S(1)} %copy-done.20), channel_id=1, source_target_pairs={{0,4},{4,0},{1,5},{5,1},{2,6},{6,2},{3,7},{7,3},{8,12},{12,8},{9,1... | collective-permute-start | bytes 1105928 | tf_op jit(solution)/shard_map/ppermute | solution.py:212
  134.6 26.3 %collective-permute-start.16 = (bf16[2,768,256]{2,1,0:T(8,128)(2,1)S(1)}, bf16[2,768,256]{2,1,0:T(8,128)(2,1)S(1)}, u32[]{:S(2)}, u32[]{:S(2)}) collective-permute-start(bf16[2,768,256]{2,1,0:T(8,128)(2,1)S(1)} %slice_bitcast_fusion.7), channel_id=1, source_target_pairs={{0,4},{4,0},{1,5},{5,1},{2,6},{6,2},{3,7},{7,3},{8,12},{12,8},{9,1... | collective-permute-start | bytes 2359304 | tf_op jit(solution)/shard_map/ppermute | solution.py:212
  135.3 12.1 %collective-permute-start.14 = (bf16[768,256]{1,0:T(8,128)(2,1)S(1)}, bf16[768,256]{1,0:T(8,128)(2,1)S(1)}, u32[]{:S(2)}, u32[]{:S(2)}) collective-permute-start(bf16[768,256]{1,0:T(8,128)(2,1)S(1)} %slice_bitcast_fusion.11), channel_id=1, source_target_pairs={{0,2},{2,0},{1,3},{3,1},{4,6},{6,4},{5,7},{7,5},{8,10},{10,8},{9,1... | collective-permute-start | bytes 1179656 | tf_op jit(solution)/shard_map/ppermute | solution.py:212
  137.2 28.2 %collective-permute-start.7 = (bf16[768,256]{1,0:T(8,128)(2,1)S(1)}, bf16[768,256]{1,0:T(8,128)(2,1)S(1)}, u32[]{:S(2)}, u32[]{:S(2)}) collective-permute-start(bf16[768,256]{1,0:T(8,128)(2,1)S(1)} %fusion.15), channel_id=1, source_target_pairs={{0,2},{2,0},{1,3},{3,1},{4,6},{6,4},{5,7},{7,5},{8,10},{10,8},{9,1... | collective-permute-start | bytes 1179656 | tf_op jit(solution)/shard_map/ppermute | solution.py:212
  147.4 21.0 %collective-permute-start.15 = (bf16[768,256]{1,0:T(8,128)(2,1)S(1)}, bf16[768,256]{1,0:T(8,128)(2,1)S(1)}, u32[]{:S(2)}, u32[]{:S(2)}) collective-permute-start(bf16[768,256]{1,0:T(8,128)(2,1)S(1)} %fusion.12), channel_id=1, source_target_pairs={{0,4},{4,0},{1,5},{5,1},{2,6},{6,2},{3,7},{7,3},{8,12},{12,8},{9,1... | collective-permute-start | bytes 1179656 | tf_op jit(solution)/shard_map/ppermute | solution.py:212
  161.2 9.5 %collective-permute-start.17 = (bf16[768,256]{1,0:T(8,128)(2,1)S(1)}, bf16[768,256]{1,0:T(8,128)(2,1)S(1)}, u32[]{:S(2)}, u32[]{:S(2)}) collective-permute-start(bf16[768,256]{1,0:T(8,128)(2,1)S(1)} %fusion.16), channel_id=1, source_target_pairs={{0,2},{2,0},{1,3},{3,1},{4,6},{6,4},{5,7},{7,5},{8,10},{10,8},{9,1... | collective-permute-start | bytes 1179656 | tf_op jit(solution)/shard_map/ppermute | solution.py:212
  162.7 17.4 %collective-permute-start.27 = (bf16[720,256]{1,0:T(8,128)(2,1)S(1)}, bf16[720,256]{1,0:T(8,128)(2,1)S(1)}, u32[]{:S(2)}, u32[]{:S(2)}) collective-permute-start(bf16[720,256]{1,0:T(8,128)(2,1)S(1)} %collective-permute-done.26), channel_id=1, source_target_pairs={{0,8},{8,16},{16,24},{1,9},{9,17},{17,25},{2,10},{10,18},{18,26},{... | collective-permute-start | bytes 1105928 | tf_op jit(solution)/shard_map/ppermute | solution.py:52
  164.0 29.9 %collective-permute-start.28 = (bf16[720,256]{1,0:T(8,128)(2,1)S(1)}, bf16[720,256]{1,0:T(8,128)(2,1)S(1)}, u32[]{:S(2)}, u32[]{:S(2)}) collective-permute-start(bf16[720,256]{1,0:T(8,128)(2,1)S(1)} %collective-permute-done.26), channel_id=1, source_target_pairs={{8,0},{16,8},{24,16},{9,1},{17,9},{25,17},{10,2},{18,10},{26,18},{... | collective-permute-start | bytes 1105928 | tf_op jit(solution)/shard_map/ppermute | solution.py:53
  165.3 30.0 %collective-permute-start.24 = (bf16[720,256]{1,0:T(8,128)(2,1)}, bf16[720,256]{1,0:T(8,128)(2,1)S(1)}, u32[]{:S(2)}, u32[]{:S(2)}) collective-permute-start(bf16[720,256]{1,0:T(8,128)(2,1)} %collective-permute-done.4), channel_id=1, source_target_pairs={{8,16},{16,24},{9,17},{17,25},{10,18},{18,26},{11,19},{19,27},{12,... | collective-permute-start | bytes 1105928 | tf_op jit(solution)/shard_map/ppermute | solution.py:52
  168.4 45.3 %collective-permute-start.22 = (bf16[720,256]{1,0:T(8,128)(2,1)}, bf16[720,256]{1,0:T(8,128)(2,1)S(1)}, u32[]{:S(2)}, u32[]{:S(2)}) collective-permute-start(bf16[720,256]{1,0:T(8,128)(2,1)} %collective-permute-done.5), channel_id=1, source_target_pairs={{8,0},{16,8},{9,1},{17,9},{10,2},{18,10},{11,3},{19,11},{12,4},{20... | collective-permute-start | bytes 1105928 | tf_op jit(solution)/shard_map/ppermute | solution.py:53
  170.8 10.8 %copy-start.26 = (f32[2,1408]{1,0:T(2,128)S(1)}, f32[2,1408]{1,0:T(2,128)}, u32[]{:S(2)}) copy-start(f32[2,1408]{1,0:T(2,128)} %param.28) | copy-start | bytes 33796
  171.7 68.7 %collective-permute-start.18 = (bf16[768,512]{1,0:T(8,128)(2,1)S(1)}, bf16[768,512]{1,0:T(8,128)(2,1)}, u32[]{:S(2)}, u32[]{:S(2)}) collective-permute-start(bf16[768,512]{1,0:T(8,128)(2,1)S(1)} %fusion.3.b0), channel_id=1, source_target_pairs={{0,2},{2,0},{1,3},{3,1},{4,6},{6,4},{5,7},{7,5},{8,10},{10,8},{9,1... | collective-permute-start | bytes 2359304 | tf_op jit(solution)/shard_map/ppermute | solution.py:212
  180.1 60.3 %copy-start.21 = (bf16[720,256]{1,0:T(8,128)(2,1)}, bf16[720,256]{1,0:T(8,128)(2,1)S(1)}, u32[]{:S(2)}) copy-start(bf16[720,256]{1,0:T(8,128)(2,1)S(1)} %collective-permute-done.27) | copy-start | bytes 1105924
  180.1 58.0 %collective-permute-start.35 = (bf16[768,512]{1,0:T(8,128)(2,1)S(1)}, bf16[768,512]{1,0:T(8,128)(2,1)}, u32[]{:S(2)}, u32[]{:S(2)}) collective-permute-start(bf16[768,512]{1,0:T(8,128)(2,1)S(1)} %fusion.3.b0), channel_id=1, source_target_pairs={{0,4},{4,0},{1,5},{5,1},{2,6},{6,2},{3,7},{7,3},{8,12},{12,8},{9,1... | collective-permute-start | bytes 2359304 | tf_op jit(solution)/shard_map/ppermute | solution.py:212
  193.9 46.5 %copy-start.23 = (bf16[720,256]{1,0:T(8,128)(2,1)}, bf16[720,256]{1,0:T(8,128)(2,1)S(1)}, u32[]{:S(2)}) copy-start(bf16[720,256]{1,0:T(8,128)(2,1)S(1)} %collective-permute-done.28) | copy-start | bytes 1105924
  193.9 20.6 %collective-permute-start.31 = (bf16[720,256]{1,0:T(8,128)(2,1)S(1)}, bf16[720,256]{1,0:T(8,128)(2,1)}, u32[]{:S(2)}, u32[]{:S(2)}) collective-permute-start(bf16[720,256]{1,0:T(8,128)(2,1)S(1)} %collective-permute-done.27), channel_id=1, source_target_pairs={{8,16},{16,24},{9,17},{17,25},{10,18},{18,26},{11,19},{19,27},{12,... | collective-permute-start | bytes 1105928 | tf_op jit(solution)/shard_map/ppermute | solution.py:52
  195.4 41.0 %collective-permute-start.29 = (bf16[720,256]{1,0:T(8,128)(2,1)S(1)}, bf16[720,256]{1,0:T(8,128)(2,1)}, u32[]{:S(2)}, u32[]{:S(2)}) collective-permute-start(bf16[720,256]{1,0:T(8,128)(2,1)S(1)} %collective-permute-done.28), channel_id=1, source_target_pairs={{8,0},{16,8},{9,1},{17,9},{10,2},{18,10},{11,3},{19,11},{12,4},{20... | collective-permute-start | bytes 1105928 | tf_op jit(solution)/shard_map/ppermute | solution.py:53
  213.7 29.6 %collective-permute-start.25 = (bf16[720,256]{1,0:T(8,128)(2,1)S(1)}, bf16[720,256]{1,0:T(8,128)(2,1)S(1)}, u32[]{:S(2)}, u32[]{:S(2)}) collective-permute-start(bf16[720,256]{1,0:T(8,128)(2,1)S(1)} %collective-permute-done.24), channel_id=1, source_target_pairs={{16,24},{17,25},{18,26},{19,27},{20,28},{21,29},{22,30},{23,31}} | collective-permute-start | bytes 1105928 | tf_op jit(solution)/shard_map/ppermute | solution.py:52
  214.5 34.5 %collective-permute-start.23 = (bf16[720,256]{1,0:T(8,128)(2,1)S(1)}, bf16[720,256]{1,0:T(8,128)(2,1)S(1)}, u32[]{:S(2)}, u32[]{:S(2)}) collective-permute-start(bf16[720,256]{1,0:T(8,128)(2,1)S(1)} %collective-permute-done.22), channel_id=1, source_target_pairs={{8,0},{9,1},{10,2},{11,3},{12,4},{13,5},{14,6},{15,7}} | collective-permute-start | bytes 1105928 | tf_op jit(solution)/shard_map/ppermute | solution.py:53
  236.3 15.9 %collective-permute-start.32 = (bf16[720,256]{1,0:T(8,128)(2,1)}, bf16[720,256]{1,0:T(8,128)(2,1)S(1)}, u32[]{:S(2)}, u32[]{:S(2)}) collective-permute-start(bf16[720,256]{1,0:T(8,128)(2,1)} %collective-permute-done.31), channel_id=1, source_target_pairs={{16,24},{17,25},{18,26},{19,27},{20,28},{21,29},{22,30},{23,31}} | collective-permute-start | bytes 1105928 | tf_op jit(solution)/shard_map/ppermute | solution.py:52
  238.1 18.0 %collective-permute-start.30 = (bf16[720,256]{1,0:T(8,128)(2,1)}, bf16[720,256]{1,0:T(8,128)(2,1)S(1)}, u32[]{:S(2)}, u32[]{:S(2)}) collective-permute-start(bf16[720,256]{1,0:T(8,128)(2,1)} %collective-permute-done.29), channel_id=1, source_target_pairs={{8,0},{9,1},{10,2},{11,3},{12,4},{13,5},{14,6},{15,7}} | collective-permute-start | bytes 1105928 | tf_op jit(solution)/shard_map/ppermute | solution.py:53
  240.4 8.7 %collective-permute-start.36 = (bf16[768,256]{1,0:T(8,128)(2,1)S(1)}, bf16[768,256]{1,0:T(8,128)(2,1)S(1)}, u32[]{:S(2)}, u32[]{:S(2)}) collective-permute-start(bf16[768,256]{1,0:T(8,128)(2,1)S(1)} %slice.280), channel_id=1, source_target_pairs={{0,2},{2,0},{1,3},{3,1},{4,6},{6,4},{5,7},{7,5},{8,10},{10,8},{9,1... | collective-permute-start | bytes 1179656 | tf_op jit(solution)/shard_map/ppermute | solution.py:212
  243.4 7.8 %collective-permute-start.37 = (bf16[768,256]{1,0:T(8,128)(2,1)S(1)}, bf16[768,256]{1,0:T(8,128)(2,1)S(1)}, u32[]{:S(2)}, u32[]{:S(2)}) collective-permute-start(bf16[768,256]{1,0:T(8,128)(2,1)S(1)} %slice.281), channel_id=1, source_target_pairs={{0,4},{4,0},{1,5},{5,1},{2,6},{6,2},{3,7},{7,3},{8,12},{12,8},{9,1... | collective-permute-start | bytes 1179656 | tf_op jit(solution)/shard_map/ppermute | solution.py:212
  246.0 6.0 %copy-start.14 = (bf16[720,256]{1,0:T(8,128)(2,1)S(1)}, bf16[720,256]{1,0:T(8,128)(2,1)}, u32[]{:S(2)}) copy-start(bf16[720,256]{1,0:T(8,128)(2,1)} %copy-done.13) | copy-start | bytes 1105924
  249.0 9.0 %collective-permute-start.38 = (bf16[768,512]{1,0:T(8,128)(2,1)}, bf16[768,512]{1,0:T(8,128)(2,1)}, u32[]{:S(2)}, u32[]{:S(2)}) collective-permute-start(bf16[768,512]{1,0:T(8,128)(2,1)} %collective-permute-done.35.b0), channel_id=1, source_target_pairs={{0,1},{1,0},{2,3},{3,2},{4,5},{5,4},{6,7},{7,6},{8,9},{9,8},{10,11... | collective-permute-start | bytes 2359304 | tf_op jit(solution)/shard_map/ppermute | solution.py:212
  252.0 6.1 %collective-permute-start.39 = (bf16[768,512]{1,0:T(8,128)(2,1)}, bf16[768,512]{1,0:T(8,128)(2,1)}, u32[]{:S(2)}, u32[]{:S(2)}) collective-permute-start(bf16[768,512]{1,0:T(8,128)(2,1)} %constant_dynamic-update-slice_fusion.2.b1), channel_id=1, source_target_pairs={{0,1},{1,0},{2,3},{3,2},{4,5},{5,4},{6,7},{7,6},{8,9},{9,8},{10,11... | collective-permute-start | bytes 2359304 | tf_op jit(solution)/shard_map/ppermute | solution.py:212
  252.0 4.1 %copy-start.22 = (bf16[720,256]{1,0:T(8,128)(2,1)S(1)}, bf16[720,256]{1,0:T(8,128)(2,1)}, u32[]{:S(2)}) copy-start(bf16[720,256]{1,0:T(8,128)(2,1)} %copy-done.21) | copy-start | bytes 1105924
  257.5 16.8 %collective-permute-start.19 = (bf16[768,512]{1,0:T(8,128)(2,1)S(1)}, bf16[768,512]{1,0:T(8,128)(2,1)}, u32[]{:S(2)}, u32[]{:S(2)}) collective-permute-start(bf16[768,512]{1,0:T(8,128)(2,1)S(1)} %fusion.3.b0), channel_id=1, source_target_pairs={{0,1},{1,0},{2,3},{3,2},{4,5},{5,4},{6,7},{7,6},{8,9},{9,8},{10,11... | collective-permute-start | bytes 2359304 | tf_op jit(solution)/shard_map/ppermute | solution.py:212
  257.6 16.8 %collective-permute-start.20 = (bf16[768,512]{1,0:T(8,128)(2,1)}, bf16[768,512]{1,0:T(8,128)(2,1)}, u32[]{:S(2)}, u32[]{:S(2)}) collective-permute-start(bf16[768,512]{1,0:T(8,128)(2,1)} %collective-permute-done.18.b1), channel_id=1, source_target_pairs={{0,1},{1,0},{2,3},{3,2},{4,5},{5,4},{6,7},{7,6},{8,9},{9,8},{10,11... | collective-permute-start | bytes 2359304 | tf_op jit(solution)/shard_map/ppermute | solution.py:212
  258.1 2.6 copy-start.2
  260.7 9.8 %copy-start.1 = (bf16[4,720,256]{2,1,0:T(8,128)(2,1)S(1)}, bf16[4,720,256]{2,1,0:T(8,128)(2,1)}, u32[]{:S(2)}) copy-start(bf16[4,720,256]{2,1,0:T(8,128)(2,1)} %pad_maximum_fusion.1.late) | copy-start | bytes 4423684
  270.5 3.9 %copy-start.3 = (bf16[8,256,1408]{2,1,0:T(8,128)(2,1)S(1)}, bf16[8,256,1408]{2,1,0:T(8,128)(2,1)}, u32[]{:S(2)}) copy-start(bf16[8,256,1408]{2,1,0:T(8,128)(2,1)} %all-gather.7.cloned.1.call-done) | copy-start | bytes 17301508
  274.3 14.2 %collective-permute-start.40 = (bf16[2,2,768,256]{3,2,1,0:T(8,128)(2,1)S(1)}, bf16[2,2,768,256]{3,2,1,0:T(8,128)(2,1)S(1)}, u32[]{:S(2)}, u32[]{:S(2)}) collective-permute-start(bf16[2,2,768,256]{3,2,1,0:T(8,128)(2,1)S(1)} %get-tuple-element.28), channel_id=1, source_target_pairs={{0,1},{1,0},{2,3},{3,2},{4,5},{5,4},{6,7},{7,6},{8,9},{9,8},{10,11... | collective-permute-start | bytes 4718600 | tf_op jit(solution)/shard_map/ppermute | solution.py:212
  288.0 4.2 %collective-permute-start.33 = (bf16[2,2,768,256]{3,2,0,1:T(8,128)(2,1)S(1)}, bf16[2,2,768,256]{3,2,0,1:T(8,128)(2,1)S(1)}, u32[]{:S(2)}, u32[]{:S(2)}) collective-permute-start(bf16[2,2,768,256]{3,2,0,1:T(8,128)(2,1)S(1)} %copy.27), channel_id=1, source_target_pairs={{0,1},{1,0},{2,3},{3,2},{4,5},{5,4},{6,7},{7,6},{8,9},{9,8},{10,11... | collective-permute-start | bytes 4718600 | tf_op jit(solution)/shard_map/ppermute | solution.py:212
  289.0 20.5 %collective-permute-start.43 = (bf16[2,768,256]{2,1,0:T(8,128)(2,1)S(1)}, bf16[2,768,256]{2,1,0:T(8,128)(2,1)S(1)}, u32[]{:S(2)}, u32[]{:S(2)}) collective-permute-start(bf16[2,768,256]{2,1,0:T(8,128)(2,1)S(1)} %slice_bitcast_fusion.3), channel_id=1, source_target_pairs={{0,4},{4,0},{1,5},{5,1},{2,6},{6,2},{3,7},{7,3},{8,12},{12,8},{9,1... | collective-permute-start | bytes 2359304 | tf_op jit(solution)/shard_map/ppermute | solution.py:212
  290.7 12.1 %collective-permute-start.41 = (bf16[768,256]{1,0:T(8,128)(2,1)S(1)}, bf16[768,256]{1,0:T(8,128)(2,1)S(1)}, u32[]{:S(2)}, u32[]{:S(2)}) collective-permute-start(bf16[768,256]{1,0:T(8,128)(2,1)S(1)} %slice_bitcast_fusion.10), channel_id=1, source_target_pairs={{0,2},{2,0},{1,3},{3,1},{4,6},{6,4},{5,7},{7,5},{8,10},{10,8},{9,1... | collective-permute-start | bytes 1179656 | tf_op jit(solution)/shard_map/ppermute | solution.py:212
  292.6 18.7 %collective-permute-start.34 = (bf16[768,256]{1,0:T(8,128)(2,1)S(1)}, bf16[768,256]{1,0:T(8,128)(2,1)S(1)}, u32[]{:S(2)}, u32[]{:S(2)}) collective-permute-start(bf16[768,256]{1,0:T(8,128)(2,1)S(1)} %fusion.17), channel_id=1, source_target_pairs={{0,2},{2,0},{1,3},{3,1},{4,6},{6,4},{5,7},{7,5},{8,10},{10,8},{9,1... | collective-permute-start | bytes 1179656 | tf_op jit(solution)/shard_map/ppermute | solution.py:212
  302.8 14.1 %collective-permute-start.42 = (bf16[768,256]{1,0:T(8,128)(2,1)S(1)}, bf16[768,256]{1,0:T(8,128)(2,1)S(1)}, u32[]{:S(2)}, u32[]{:S(2)}) collective-permute-start(bf16[768,256]{1,0:T(8,128)(2,1)S(1)} %fusion.7), channel_id=1, source_target_pairs={{0,4},{4,0},{1,5},{5,1},{2,6},{6,2},{3,7},{7,3},{8,12},{12,8},{9,1... | collective-permute-start | bytes 1179656 | tf_op jit(solution)/shard_map/ppermute | solution.py:212
  309.7 9.3 %collective-permute-start.44 = (bf16[768,256]{1,0:T(8,128)(2,1)S(1)}, bf16[768,256]{1,0:T(8,128)(2,1)S(1)}, u32[]{:S(2)}, u32[]{:S(2)}) collective-permute-start(bf16[768,256]{1,0:T(8,128)(2,1)S(1)} %fusion.18), channel_id=1, source_target_pairs={{0,2},{2,0},{1,3},{3,1},{4,6},{6,4},{5,7},{7,5},{8,10},{10,8},{9,1... | collective-permute-start | bytes 1179656 | tf_op jit(solution)/shard_map/ppermute | solution.py:212
  (12 other events, 20.5 us)
Sparse Core Ops, SparseCore 0:
  30.6 81.0 all-gather.4
  113.3 128.5 all-gather.6
where the time goes:
time: 330 us; the launch traced here: 327 us
  waiting for transfers between devices  183 us (55%)
  starting transfers between devices  50.7 us (15%)
  Pallas kernels  45 us (14%)
  local copies, waits for them, and re-layouts  18.2 us (6%)
  other arithmetic  15.9 us (5%)
  between operations  14.4 us (4%)
    ppermute x33, waiting for transfers between devices, swap(): return lax.ppermute(values, axis, PAIR)  84.2 us
    ppermute x6, waiting for transfers between devices, line_hop(): lax.ppermute(down, 'z', [(i, i - 1) for i in range(1, n - step + 1)])  59 us
    pallas_call x6, Pallas kernels, call(): pl.pallas_call(kernel, grid_spec=pltpu.PrefetchScalarGridSpec(num_scalar_...  45 us
    ppermute x33, starting transfers between devices, swap(): return lax.ppermute(values, axis, PAIR)  33.7 us
    all_gather x1, waiting for transfers between devices, on_device(): mixer_w = lax.all_gather(mixer_own, 'z')  33.1 us
    ppermute x6, starting transfers between devices, line_hop(): lax.ppermute(up, 'z', [(i, i + 1) for i in range(step - 1, n - 1)])  9.01 us
    unnamed x60, local copies, waits for them, and re-layouts  7.93 us
    ppermute x6, starting transfers between devices, line_hop(): lax.ppermute(down, 'z', [(i, i - 1) for i in range(1, n - step + 1)])  7.9 us
  transfers between devices with their start and end apart: 47, of which 22 were waited for; matrix products, arithmetic and copies ran while one was open for 7% of the time, Pallas kernels for 14%

commit v1 on v0

--- a/solution.py
+++ b/solution.py
@@ -45,26 +45,14 @@
     return out
 
 
-def line_hop(chunks, step):
-    n = lax.axis_size("z")
-    up, down = chunks
-    return (
-        lax.ppermute(up, "z", [(i, i + 1) for i in range(step - 1, n - 1)]),
-        lax.ppermute(down, "z", [(i, i - 1) for i in range(1, n - step + 1)]),
-    )
-
-
-def line_order(hops):
+def line_gather(chunk):
     n = lax.axis_size("z")
     own = lax.axis_index("z")
-    return [hops[0][0]] + [jnp.where(own >= s, hops[s][0], hops[n - s][1]) for s in range(1, n)]
-
-
-def line_gather(chunk):
-    hops = [(chunk, chunk)]
-    for step in range(1, lax.axis_size("z")):
-        hops.append(line_hop(hops[-1], step))
-    return line_order(hops)
+    ups, downs = [chunk], [chunk]
+    for s in range(1, n):
+        ups.append(lax.ppermute(ups[-1], "z", [(i, i + 1) for i in range(s - 1, n - 1)]))
+        downs.append(lax.ppermute(downs[-1], "z", [(i, i - 1) for i in range(1, n - s + 1)]))
+    return [chunk] + [jnp.where(own >= s, ups[s], downs[n - s]) for s in range(1, n)]
 
 
 def gather_weight(parts):
@@ -225,7 +213,7 @@
         out_shape=out_shape,
         cost_estimate=pl.CostEstimate(flops=flops, bytes_accessed=8 << 20, transcendentals=0),
         compiler_params=pltpu.CompilerParams(
-            dimension_semantics=("arbitrary",), vmem_limit_bytes=30 << 20
+            dimension_semantics=("arbitrary",), vmem_limit_bytes=(16 if kernel is down_kernel else 28) << 20
         ),
     )(order, *arrays)
 
@@ -248,17 +236,19 @@
     return total
 
 
-def norm_into(order, blocks, gain, rows):
+def norm_into(order, blocks, gain, rows, place):
     squares = 0.0
     for block in blocks:
         floats = block[...].astype(jnp.float32)
         squares = squares + jnp.sum(floats * floats, axis=-1, keepdims=True)
     width = blocks[0].shape[-1]
+    half = width // 2
     factor = lax.rsqrt(squares / (width * len(blocks)) + EPS)
     for j, block in enumerate(blocks):
-        normed = block[...].astype(jnp.float32) * factor * gain[order[j]]
-        at = pl.multiple_of(order[j] * width, LANES)
-        rows[:, pl.ds(at, width)] = normed.astype(jnp.bfloat16)
+        normed = (block[...].astype(jnp.float32) * factor * gain[order[j]]).astype(jnp.bfloat16)
+        for h in range(2):
+            at = pl.multiple_of(place(j, h) * half, LANES)
+            rows[:, pl.ds(at, half)] = normed[:, h * half : (h + 1) * half]
 
 
 def scaled_terms(acts, matrix, scale):
@@ -268,28 +258,39 @@
     return (part * total).astype(jnp.bfloat16)
 
 
-def mixer_kernel(order, b0, b1, b2, b3, gain, weights, scales, taps, keep, send, rows):
-    norm_into(order, (b0, b1, b2, b3), gain, rows)
-    width = weights.shape[-1]
-    unit = weights.shape[0] * weights.shape[1]
-    k = rows.shape[1] // unit
+def mixer_kernel(order, b0, b1, b2, b3, gain, *refs):
+    *slabs, scales, taps, keep, send, rows, last = refs
+    width = slabs[0].shape[-1]
+    k = rows.shape[1] // len(slabs)
+    low = 3 * k
+    y = order[8]
+
+    @pl.when(pl.program_id(0) == 0)
+    def _():
+        for q, slab in enumerate(slabs):
+            last[q] = slab[low:, :]
+
+    norm_into(order, (b0, b1, b2, b3), gain, rows, lambda j, h: 2 * order[4 + j] + (h + y) % 2)
 
     def project(m):
-        matrix = weights[:, :, m * k : (m + 1) * k, :].reshape(unit * k, width)
-        result = jnp.dot(rows[...], matrix, preferred_element_type=jnp.float32)
+        result = 0.0
+        for q, slab in enumerate(slabs):
+            acts = rows[:, q * k : (q + 1) * k]
+            matrix = slab[m * k : (m + 1) * k, :]
+            result = result + jnp.dot(acts, matrix, preferred_element_type=jnp.float32)
         return result * scales[m : m + 1]
 
     inner = project(1) * project(2)
     gated = (project(0) * conv_rows(inner, taps[...])).astype(jnp.bfloat16)
-    low = 3 * k
     for j in range(4):
         for h in range(2):
-            matrix, scale = weights[order[j], h, low : low + width, :], weights[order[j], h, low + width :, :]
-            (keep, send)[j // 2][j % 2, h] = scaled_terms(gated, matrix, scale)
+            at = 2 * order[4 + j] + (h + y) % 2
+            terms = scaled_terms(gated, last[at, :width, :], last[at, width:, :])
+            (keep, send)[j // 2][j % 2, h] = terms
 
 
 def up_kernel(order, b0, b1, b2, b3, gain, weights, scales, taps, active, rows):
-    norm_into(order, (b0, b1, b2, b3), gain, rows)
+    norm_into(order, (b0, b1, b2, b3), gain, rows, lambda j, h: 2 * order[j] + h)
     both = weights.shape[-1]
     hidden = both // 2
     matrix = weights[...].reshape(rows.shape[1], both)
@@ -305,13 +306,13 @@
         active[:, full:] = part[:, : hidden - full].astype(jnp.bfloat16)
 
 
-def down_kernel(order, active, early, late, keep, send):
+def down_kernel(order, active, weights, keep, send):
     acts = active[...]
     hidden = acts.shape[1]
     for j in range(4):
-        for i, weights in enumerate((late, early)):
-            matrix, scale = weights[order[j], :hidden, :], weights[order[j], hidden:, :]
-            (keep, send)[j // 2][j % 2, order[4 + i]] = scaled_terms(acts, matrix, scale)
+        for h in range(2):
+            matrix, scale = weights[order[j], h, :hidden, :], weights[order[j], h, hidden:, :]
+            (keep, send)[j // 2][j % 2, h] = scaled_terms(acts, matrix, scale)
 
 
 def term_shapes(seqs, length, width):
@@ -321,12 +322,15 @@
     return (shape, shape), (spec, spec)
 
 
-def plane_blocks(own):
+def plane_blocks(own, both=True):
     half = own.shape[1] // 2
-    across, beside = swap(own, "x"), swap(own, "y")
+    across = swap(own, "x")
+    beside = swap(own, "y")
     twin = swap(own, "c")
-    left, right = swap(beside[:, :half], "x"), swap(across[:, half:], "y")
-    corner = jnp.concatenate([left, right], axis=1)
+    if both:
+        corner = jnp.concatenate([swap(beside[:, :half], "x"), swap(across[:, half:], "y")], axis=1)
+    else:
+        corner = swap(beside, "x")
     mine = (own, across, twin, swap(across, "c"))
     theirs = (beside, corner, swap(beside, "c"), swap(corner, "c"))
     return mine, theirs
@@ -348,7 +352,8 @@
     left_far = far[0, 0] + moved(far[1, 0], "x")
     right = near[:, 1] + moved(far[:, 1], "y")
     left_near = near[0, 0] + moved(near[1, 0], "x")
-    left, right = left_near + moved(left_far, "y"), right[0] + moved(right[1], "x")
+    left = left_near + moved(left_far, "y")
+    right = right[0] + moved(right[1], "x")
     return jnp.concatenate([left, right], axis=1)
 
 
@@ -395,39 +400,46 @@
         return jnp.concatenate(split_terms(scale) + [spare])
 
     z = lax.axis_index("z")
+    inside = (z == 1) | (z == 2)
     own = tokens.reshape(row_count, own_width)
+    outer = lax.ppermute(own, "z", [(0, 1), (3, 2)])
 
     ins = [halves(rounded(m), 1) for m in (w_bgate, w_cgate, w_value)]
     outs = halves(rounded(w_mixout), 0)
     mix_rows, down_rows = scale_rows(mixout_scale), scale_rows(down_scale)
-    downs = [jnp.concatenate([d, down_rows]) for d in halves(rounded(w_down), 0)]
-    early = pick(downs, y)
-    hops = [(early, early)]
-    hops.append(line_hop(hops[-1], 1))
-    mixer_own = exchanged(*(jnp.concatenate([m[i] for m in ins] + [outs[i], mix_rows]) for i in range(2)))
-    mixer_own, hops = lax.optimization_barrier((mixer_own, hops))
-    mixer_w = lax.all_gather(mixer_own, "z")
-    hops.append(line_hop(hops[-1], 2))
-    hops.append(line_hop(hops[-1], 3))
-    early_w = jnp.stack(line_order(hops))
+    mixer_halves = [jnp.concatenate([m[i] for m in ins] + [outs[i], mix_rows]) for i in range(2)]
+    mixer_keep = pick(mixer_halves, y)
+    mixer_got = swap(pick(mixer_halves[::-1], y), "y")
+
+    def to_inside(chunk):
+        below = lax.ppermute(chunk, "z", [(0, 1), (1, 2)])
+        above = lax.ppermute(chunk, "z", [(3, 2), (2, 1)])
+        from_first = lax.ppermute(below, "z", [(1, 2)])
+        from_last = lax.ppermute(above, "z", [(2, 1)])
+        return chunk, below, above, jnp.where(z == 1, from_last, from_first)
+
+    kept, gotten = to_inside(mixer_keep), to_inside(mixer_got)
+    slabs = tuple(s for pair in zip(kept, gotten) for s in pair)
+    origins = [(z + d) % blocks for d in (0, -1, 1, 2)]
+
     ups = [
         packed(g, v) for g, v in zip(halves(rounded(w_upgate), 1), halves(rounded(w_upval), 1))
     ]
     up_own = exchanged(*ups)
+    near, far = plane_blocks(own, False)
+    outer_near, outer_far = plane_blocks(outer, False)
+    up_own, slabs = lax.optimization_barrier((up_own, slabs))
     up_w = lax.all_gather(up_own, "z")
-    late = swap(pick(downs[::-1], y), "y")
-    late_hops = [(late, late)]
-    for step in (1, 2, 3):
-        late_hops.append(line_hop(late_hops[-1], step))
-    late_w = jnp.stack(line_order(late_hops))
-
     places = [jx * 2 + jc for jc in (c, 1 - c) for jx in (x, 1 - x)]
+
+    def index_of(value, entries):
+        return sum(jnp.where(value == e, i, 0) for i, e in enumerate(entries))
 
     def table(*entries):
         return jnp.stack(entries).astype(jnp.int32)
 
-    order = table(*places)
-    down_order = table(*((z - t) % blocks for t in places), 1 - y, y)
+    mixer_order = table(*places, *(index_of(t, origins) for t in places), y)
+    up_order = table(*places, *places)
 
     def mine(values, axis):
         return pick(halves(values, axis), y)
@@ -439,13 +451,15 @@
     rows_scratch = [pltpu.VMEM((length, features), jnp.bfloat16)]
 
     def mixer(group):
-        width = mixer_w.shape[-1]
-        small = (mix_gain.reshape(blocks, 1, own_width), mixer_w, mine(in_scale, 1), mine(mix_taps, 1))
+        width = mixer_keep.shape[-1]
+        small = (mix_gain.reshape(blocks, 1, own_width), *slabs, mine(in_scale, 1), mine(mix_taps, 1))
         shapes, specs = term_shapes(seqs, length, width)
         flops = 2 * row_count * features * width * 4
+        rest = mixer_keep.shape[0] - 3 * w_mixout.shape[1]
+        scratch = rows_scratch + [pltpu.VMEM((2 * blocks, rest, width), jnp.bfloat16)]
         return call(
             mixer_kernel, (seqs,), block_specs(own_width) + [whole(a) for a in small], specs, shapes,
-            rows_scratch, flops, order, *group, *small,
+            scratch, flops, mixer_order, *group, *small,
         )
 
     def up(group):
@@ -458,27 +472,38 @@
             up_kernel, (seqs,), block_specs(own_width) + [whole(a) for a in small],
             pl.BlockSpec((length, hidden), lambda i, order: (i, 0)),
             jax.ShapeDtypeStruct((row_count, hidden), jnp.bfloat16),
-            rows_scratch, flops, order, *group, *small,
+            rows_scratch, flops, up_order, *group, *small,
         )
 
     def down(active):
         hidden = active.shape[1]
-        shapes, specs = term_shapes(seqs, length, early_w.shape[-1])
+        shapes, specs = term_shapes(seqs, length, down_w.shape[-1])
         flops = 2 * row_count * features * hidden
         return call(
             down_kernel, (seqs,),
-            [pl.BlockSpec((length, hidden), lambda i, order: (i, 0)), whole(early_w), whole(late_w)],
-            specs, shapes, [], flops, down_order, active, early_w, late_w,
+            [pl.BlockSpec((length, hidden), lambda i, order: (i, 0)), whole(down_w)],
+            specs, shapes, [], flops, up_order, active, down_w,
         )
 
     def added(base, sums):
         return (base.astype(jnp.float32) + sums).astype(jnp.bfloat16)
 
-    near, far = plane_blocks(own)
+    terms_far = mixer(outer_far)
+    outer_near, terms_far = lax.optimization_barrier((outer_near, terms_far))
+    terms_near = mixer(outer_near)
+    near, far, terms_near = lax.optimization_barrier((near, far, terms_near))
+    outer_out = added(outer, plane_sums(terms_near, terms_far))
+    back = lax.ppermute(outer_out, "z", [(1, 0), (2, 3)])
     terms_far = mixer(far)
+    near, terms_far, w_down, down_rows = lax.optimization_barrier((near, terms_far, w_down, down_rows))
+    downs = [jnp.concatenate([d, down_rows]) for d in halves(rounded(w_down), 0)]
+    down_own = exchanged(*downs)
+    down_w = lax.all_gather(down_own, "z")
     resid = added(own, plane_sums(mixer(near), terms_far))
+    resid = jnp.where(inside, resid, back)
     near, far = plane_blocks(resid)
-    active_near, active_far = up(near), up(far)
+    active_near = up(near)
+    active_far = up(far)
     terms_far = down(active_far)
     layer_out = added(resid, plane_sums(down(active_near), terms_far))
     return layer_out.reshape(seqs, length, own_width)

time: 330 us -> 422 us (1.28)
  starting transfers between devices: 50.7 us -> 81.3 us
  waiting for transfers between devices: 183 us -> 206 us
  Pallas kernels: 45 us -> 67.2 us
  other arithmetic: 15.9 us -> 25.6 us
  local copies, waits for them, and re-layouts: 18.2 us -> 26.8 us
    ppermute x33 -> x46, waiting for transfers between devices: 84.2 us -> 163 us  [swap(): return lax.ppermute(values, axis, PAIR)]
    all_gather x1, waiting for transfers between devices: 33.1 us -> 0.01 us  [on_device(): down_w = lax.all_gather(down_own, 'z')]
    ppermute x12 -> x10, starting transfers between devices: 16.9 us -> 43.4 us  [the longest x1 27.9 us: on_device(): outer = lax.ppermute(own, 'z', [(0, 1), (3, 2)])]
    ppermute x12 -> x10, waiting for transfers between devices: 65.8 us -> 43 us  [the longest x1 27.9 us: on_device(): outer = lax.ppermute(own, 'z', [(0, 1), (3, 2)])]
    pallas_call x6 -> x8, Pallas kernels: 45 us -> 67.2 us  [call(): pl.pallas_call(kernel, grid_spec=pltpu.PrefetchScalarGridSpec(num_scalar_...]
    unnamed x60 -> x115, local copies, waits for them, and re-layouts: 7.93 us -> 22.7 us
    add x4 -> x6, other arithmetic: 1.43 us -> 7.93 us  [over_cores(): return keep.astype(jnp.float32) + got.astype(jnp.float32)]
    select_n x0 -> x3, other arithmetic: none -> 4.44 us  [the longest x2 2.78 us: to_inside(): return (chunk, below, above, jnp.where(z == 1, from_last, from_first))]
  transfers between devices with their start and end apart: 47 -> 58, of which waited for: 22 -> 25; matrix products, arithmetic and copies ran while one was open for 7% -> 6% of each run, Pallas kernels for 14% -> 16%
where the time goes in v1:
time: 422 us; the launch traced here: 421 us
  waiting for transfers between devices  206 us (49%)
  starting transfers between devices  81.3 us (19%)
  Pallas kernels  67.2 us (16%)
  local copies, waits for them, and re-layouts  26.8 us (6%)
  other arithmetic  25.6 us (6%)
  between operations  14.4 us (3%)
    ppermute x46, waiting for transfers between devices, swap(): return lax.ppermute(values, axis, PAIR)  163 us
    pallas_call x8, Pallas kernels, call(): pl.pallas_call(kernel, grid_spec=pltpu.PrefetchScalarGridSpec(num_scalar_...  67.2 us
    ppermute x46, starting transfers between devices, swap(): return lax.ppermute(values, axis, PAIR)  37.8 us
    ppermute x1, waiting for transfers between devices, on_device(): outer = lax.ppermute(own, 'z', [(0, 1), (3, 2)])  27.9 us
    ppermute x1, starting transfers between devices, on_device(): outer = lax.ppermute(own, 'z', [(0, 1), (3, 2)])  27.9 us
    unnamed x115, local copies, waits for them, and re-layouts  22.7 us
    ppermute x1, waiting for transfers between devices, on_device(): back = lax.ppermute(outer_out, 'z', [(1, 0), (2, 3)])  11.2 us
  transfers between devices with their start and end apart: 58, of which 25 were waited for; matrix products, arithmetic and copies ran while one was open for 6% of the time, Pallas kernels for 16%

profile of v1, /device:TPU:0, one launch (start us, length us, event | category | flops | bytes accessed | tf_op | source)
XLA Modules:
  0.0 421.0 jit_solution(4893248485846119244)
XLA Ops:
  6.5 1.5 convert_element_type.197
  10.2 3.0 collective-permute-start.15
  15.8 4.1 collective-permute-start.17
  19.9 21.1 %collective-permute-done.16.refs_1_ = bf16[1040,256]{1,0:T(8,128)(2,1)S(1)} collective-permute-done((bf16[1040,256]{1,0:T(8,128)(2,1)S(1)}, bf16[1040,256]{1,0:T(8,128)(2,1)S(1)}, u32[]{:S(2)}, u32[]{:S(2)}) %collective-permute-start.16) | collective-permute-done | bytes 532512 | tf_op jit(solution)/shard_map/ppermute | solution.py:200
  41.0 3.7 collective-permute-start.18
  45.4 1.5 collective-permute-start.21
  46.9 1.5 collective-permute-start.22
  48.3 1.5 select_bitcast_fusion.1
  49.9 1.5 collective-permute-start.23
  51.4 3.8 collective-permute-done.18.refs_3_
  57.1 1.9 broadcast_select_fusion.3.refs_6_
  60.0 27.9 %collective-permute-start.7 = (bf16[768,512]{1,0:T(8,128)(2,1)}, bf16[768,512]{1,0:T(8,128)(2,1)S(1)}, u32[]{:S(2)}, u32[]{:S(2)}) collective-permute-start(bf16[768,512]{1,0:T(8,128)(2,1)} %bitcast.b0), channel_id=1, source_target_pairs={{0,8},{24,16},{1,9},{25,17},{2,10},{26,18},{3,11},{27,19},{4,12},{... | collective-permute-start | bytes 2359304 | tf_op jit(solution)/shard_map/ppermute | solution.py:405
  87.9 27.9 %collective-permute-done.7.b0 = bf16[768,512]{1,0:T(8,128)(2,1)S(1)} collective-permute-done((bf16[768,512]{1,0:T(8,128)(2,1)}, bf16[768,512]{1,0:T(8,128)(2,1)S(1)}, u32[]{:S(2)}, u32[]{:S(2)}) %collective-permute-start.7) | collective-permute-done | bytes 786464 | tf_op jit(solution)/shard_map/ppermute | solution.py:405
  115.8 1.3 collective-permute-start.11
  117.8 1.3 collective-permute-start
  119.1 15.3 %collective-permute-done.11.b0 = bf16[768,512]{1,0:T(8,128)(2,1)S(1)} collective-permute-done((bf16[768,512]{1,0:T(8,128)(2,1)S(1)}, bf16[768,512]{1,0:T(8,128)(2,1)S(1)}, u32[]{:S(2)}, u32[]{:S(2)}) %collective-permute-start.11) | collective-permute-done | bytes 786464 | tf_op jit(solution)/shard_map/ppermute | solution.py:200
  134.4 1.3 collective-permute-start.12
  136.4 6.5 %collective-permute-done.3.b0 = bf16[768,512]{1,0:T(8,128)(2,1)} collective-permute-done((bf16[768,512]{1,0:T(8,128)(2,1)}, bf16[768,512]{1,0:T(8,128)(2,1)}, u32[]{:S(2)}, u32[]{:S(2)}) %collective-permute-start.3) | collective-permute-done | bytes 786464 | tf_op jit(solution)/shard_map/ppermute | solution.py:200
  142.9 1.3 collective-permute-start.4
  145.6 9.7 %collective-permute-done.12.b1 = bf16[768,512]{1,0:T(8,128)(2,1)S(1)} collective-permute-done((bf16[768,512]{1,0:T(8,128)(2,1)S(1)}, bf16[768,512]{1,0:T(8,128)(2,1)S(1)}, u32[]{:S(2)}, u32[]{:S(2)}) %collective-permute-start.12) | collective-permute-done | bytes 786464 | tf_op jit(solution)/shard_map/ppermute | solution.py:200
  156.3 14.8 %collective-permute-done.8.b1 = bf16[768,512]{1,0:T(8,128)(2,1)} collective-permute-done((bf16[768,512]{1,0:T(8,128)(2,1)S(1)}, bf16[768,512]{1,0:T(8,128)(2,1)}, u32[]{:S(2)}, u32[]{:S(2)}) %collective-permute-start.8) | collective-permute-done | bytes 786464 | tf_op jit(solution)/shard_map/ppermute | solution.py:200
  171.1 8.4 %collective-permute-done.4.b1 = bf16[768,512]{1,0:T(8,128)(2,1)} collective-permute-done((bf16[768,512]{1,0:T(8,128)(2,1)}, bf16[768,512]{1,0:T(8,128)(2,1)}, u32[]{:S(2)}, u32[]{:S(2)}) %collective-permute-start.4) | collective-permute-done | bytes 786464 | tf_op jit(solution)/shard_map/ppermute | solution.py:200
  190.2 10.2 %shard_map.154 = (bf16[2,2,768,256]{3,2,1,0:T(8,128)(2,1)S(1)}, bf16[2,2,768,256]{3,2,1,0:T(8,128)(2,1)}) custom-call(s32[9]{0:T(128)S(1)} %stack.68.order, bf16[768,512]{1,0:T(8,128)(2,1)S(1)} %copy-done.19, bf16[768,512]{1,0:T(8,128)(2,1)S(1)} %copy-done.21, bf16[768,512]{1,0:T(8,128)(2,1)} %collective-permute-done.13.b2, ...), custom_call_target="tpu_custom_call" | custom-call | flops 3221225472 | bytes 8388608 | tf_op jit(solution)/shard_map/pallas_call | solution.py:204
  202.7 9.9 %shard_map.155 = (bf16[2,2,768,256]{3,2,1,0:T(8,128)(2,1)S(1)}, bf16[2,2,768,256]{3,2,1,0:T(8,128)(2,1)}) custom-call(s32[9]{0:T(128)S(1)} %stack.68.order, bf16[768,512]{1,0:T(8,128)(2,1)S(1)} %copy-done.5, bf16[768,512]{1,0:T(8,128)(2,1)} %collective-permute-done.8.b1, bf16[768,512]{1,0:T(8,128)(2,1)} %collective-permute-done.9.b2, ...), custom_call_target="tpu_custom_call" | custom-call | flops 3221225472 | bytes 8388608 | tf_op jit(solution)/shard_map/pallas_call | solution.py:204
  212.7 9.9 %shard_map.156 = (bf16[2,2,768,256]{3,2,1,0:T(8,128)(2,1)S(1)}, bf16[2,2,768,256]{3,2,1,0:T(8,128)(2,1)}) custom-call(s32[9]{0:T(128)S(1)} %stack.68.order, bf16[768,512]{1,0:T(8,128)(2,1)} %collective-permute-done.3.b0, bf16[768,512]{1,0:T(8,128)(2,1)} %collective-permute-done.4.b1, bf16[768,512]{1,0:T(8,128)(2,1)S(1)} %collective-permute-done.5.b2, ...), custom_call_target="tpu_custom_call" | custom-call | flops 3221225472 | bytes 8388608 | tf_op jit(solution)/shard_map/pallas_call | solution.py:204
  223.9 1.4 collective-permute-start.43
  225.4 10.2 %shard_map.157 = (bf16[2,2,768,256]{3,2,1,0:T(8,128)(2,1)S(1)}, bf16[2,2,768,256]{3,2,1,0:T(8,128)(2,1)}) custom-call(s32[9]{0:T(128)S(1)} %stack.68.order, bf16[768,512]{1,0:T(8,128)(2,1)} %bitcast.b0, bf16[768,512]{1,0:T(8,128)(2,1)} %collective-permute-done.b1, bf16[768,512]{1,0:T(8,128)(2,1)S(1)} %collective-permute-done.1.b2, ...), custom_call_target="tpu_custom_call" | custom-call | flops 3221225472 | bytes 8388608 | tf_op jit(solution)/shard_map/pallas_call | solution.py:204
  238.4 1.7 convert_add_fusion.2
  242.2 1.8 convert_add_fusion.3
  245.0 1.8 convert_add_fusion.4
  246.9 1.4 collective-permute-start.30
  248.4 1.5 collective-permute-start.28
  249.9 1.7 convert_add_fusion.5
  254.3 15.6 %collective-permute-done.28 = bf16[768,256]{1,0:T(8,128)(2,1)S(1)} collective-permute-done((bf16[768,256]{1,0:T(8,128)(2,1)S(1)}, bf16[768,256]{1,0:T(8,128)(2,1)S(1)}, u32[]{:S(2)}, u32[]{:S(2)}) %collective-permute-start.28) | collective-permute-done | bytes 393248 | tf_op jit(solution)/shard_map/ppermute | solution.py:200
  269.9 1.3 collective-permute-start.36
  273.0 4.6 %collective-permute-done.30 = bf16[2,768,256]{2,1,0:T(8,128)(2,1)S(1)} collective-permute-done((bf16[2,768,256]{2,1,0:T(8,128)(2,1)S(1)}, bf16[2,768,256]{2,1,0:T(8,128)(2,1)S(1)}, u32[]{:S(2)}, u32[]{:S(2)}) %collective-permute-start.30) | collective-permute-done | bytes 786464 | tf_op jit(solution)/shard_map/ppermute | solution.py:200
  277.6 1.4 collective-permute-start.38
  279.3 6.8 %collective-permute-done.36 = bf16[768,256]{1,0:T(8,128)(2,1)S(1)} collective-permute-done((bf16[768,256]{1,0:T(8,128)(2,1)S(1)}, bf16[768,256]{1,0:T(8,128)(2,1)S(1)}, u32[]{:S(2)}, u32[]{:S(2)}) %collective-permute-start.36) | collective-permute-done | bytes 393248 | tf_op jit(solution)/shard_map/ppermute | solution.py:200
  286.1 1.4 collective-permute-done.38
  288.8 1.3 collective-permute-start.39
  290.8 1.5 collective-permute-start.31
  292.3 1.6 collective-permute-done.29
  295.0 5.4 %collective-permute-done.31 = bf16[768,256]{1,0:T(8,128)(2,1)} collective-permute-done((bf16[768,256]{1,0:T(8,128)(2,1)}, bf16[768,256]{1,0:T(8,128)(2,1)}, u32[]{:S(2)}, u32[]{:S(2)}) %collective-permute-start.31) | collective-permute-done | bytes 393248 | tf_op jit(solution)/shard_map/ppermute | solution.py:200
  301.5 11.2 %collective-permute-done.39 = bf16[768,512]{1,0:T(8,128)(2,1)} collective-permute-done((bf16[768,512]{1,0:T(8,128)(2,1)}, bf16[768,512]{1,0:T(8,128)(2,1)}, u32[]{:S(2)}, u32[]{:S(2)}) %collective-permute-start.39) | collective-permute-done | bytes 786464 | tf_op jit(solution)/shard_map/ppermute | solution.py:496
  312.7 1.7 fusion.6.b0
  314.4 1.5 collective-permute-start.46
  316.0 1.5 collective-permute-start.40
  317.4 16.3 %collective-permute-done.46.b0 = bf16[768,512]{1,0:T(8,128)(2,1)S(1)} collective-permute-done((bf16[768,512]{1,0:T(8,128)(2,1)S(1)}, bf16[768,512]{1,0:T(8,128)(2,1)S(1)}, u32[]{:S(2)}, u32[]{:S(2)}) %collective-permute-start.46) | collective-permute-done | bytes 786464 | tf_op jit(solution)/shard_map/ppermute | solution.py:200
  333.7 1.6 collective-permute-start.47
  335.3 1.3 collective-permute-start.48
  336.7 7.1 %collective-permute-done.47 = bf16[768,256]{1,0:T(8,128)(2,1)S(1)} collective-permute-done((bf16[768,256]{1,0:T(8,128)(2,1)S(1)}, bf16[768,256]{1,0:T(8,128)(2,1)S(1)}, u32[]{:S(2)}, u32[]{:S(2)}) %collective-permute-start.47) | collective-permute-done | bytes 393248 | tf_op jit(solution)/shard_map/ppermute | solution.py:200
  343.8 1.3 collective-permute-done.48
  346.3 1.3 collective-permute-done.50.b3
  347.6 2.6 copy-done.14
  350.2 10.0 %shard_map.160.active = bf16[768,704]{1,0:T(8,128)(2,1)S(1)} custom-call(s32[8]{0:T(128)S(1)} %stack.72.order, bf16[768,512]{1,0:T(8,128)(2,1)S(1)} %collective-permute-done.46.b0, bf16[768,512]{1,0:T(8,128)(2,1)S(1)} %constant_dynamic-update-slice_fusion.b1, bf16[768,512]{1,0:T(8,128)(2,1)} %collective-permute-done.49.b2, ...), custom_call_target="tpu_custom_call" | custom-call | flops 4429185024 | bytes 8388608 | tf_op jit(solution)/shard_map/pallas_call | solution.py:204
  361.3 1.8 copy-done.16
  363.1 1.3 copy-done.40
  364.4 3.6 shard_map.161
  368.2 9.9 %shard_map.158.active = bf16[768,704]{1,0:T(8,128)(2,1)S(1)} custom-call(s32[8]{0:T(128)S(1)} %stack.72.order, bf16[768,512]{1,0:T(8,128)(2,1)S(1)} %fusion.6.b0, bf16[768,512]{1,0:T(8,128)(2,1)S(1)} %collective-permute-done.40.b1, bf16[768,512]{1,0:T(8,128)(2,1)} %collective-permute-done.41.b2, bf16[768,512]{1,0:T(8,128)(2,1)} %collective-permute-done.42.b3, ...), custom_call_target="tpu_custom_call" | custom-call | flops 4429185024 | bytes 8388608 | tf_op jit(solution)/shard_map/pallas_call | solution.py:204
  378.1 3.6 shard_map.159
  386.2 9.5 %collective-permute-done.52 = bf16[768,256]{1,0:T(8,128)(2,1)S(1)} collective-permute-done((bf16[768,256]{1,0:T(8,128)(2,1)S(1)}, bf16[768,256]{1,0:T(8,128)(2,1)S(1)}, u32[]{:S(2)}, u32[]{:S(2)}) %collective-permute-start.52) | collective-permute-done | bytes 393248 | tf_op jit(solution)/shard_map/ppermute | solution.py:200
  396.8 6.1 %collective-permute-done.54 = bf16[2,768,256]{2,1,0:T(8,128)(2,1)S(1)} collective-permute-done((bf16[2,768,256]{2,1,0:T(8,128)(2,1)S(1)}, bf16[2,768,256]{2,1,0:T(8,128)(2,1)S(1)}, u32[]{:S(2)}, u32[]{:S(2)}) %collective-permute-start.54) | collective-permute-done | bytes 786464 | tf_op jit(solution)/shard_map/ppermute | solution.py:200
  404.0 6.7 %collective-permute-done.53 = bf16[768,256]{1,0:T(8,128)(2,1)S(1)} collective-permute-done((bf16[768,256]{1,0:T(8,128)(2,1)S(1)}, bf16[768,256]{1,0:T(8,128)(2,1)S(1)}, u32[]{:S(2)}, u32[]{:S(2)}) %collective-permute-start.53) | collective-permute-done | bytes 393248 | tf_op jit(solution)/shard_map/ppermute | solution.py:200
  410.8 2.2 collective-permute-done.55
  (257 shorter events, 51.6 us)
Async XLA Ops:
  6.5 341.1 %all-gather.5.cloned.1.call-start = ((), (), s32[]{:S(2)}) async-start(), calls=%async_computation | async-start | bytes 7208960 | tf_op jit(solution)/shard_map/all_gather | solution.py:432
  10.2 38.1 %collective-permute-start.15 = (bf16[256,1408]{1,0:T(8,128)(2,1)}, bf16[256,1408]{1,0:T(8,128)(2,1)}, u32[]{:S(2)}, u32[]{:S(2)}) collective-permute-start(bf16[256,1408]{1,0:T(8,128)(2,1)} %broadcast_select_fusion.1), channel_id=1, source_target_pairs={{0,4},{4,0},{1,5},{5,1},{2,6},{6,2},{3,7},{7,3},{8,12},{12,8},{9,1... | collective-permute-start | bytes 2162696 | tf_op jit(solution)/shard_map/ppermute | solution.py:200
  14.0 166.5 %copy-start.7 = (bf16[1040,256]{1,0:T(8,128)(2,1)}, bf16[1040,256]{1,0:T(8,128)(2,1)S(1)}, u32[]{:S(2)}) copy-start(bf16[1040,256]{1,0:T(8,128)(2,1)S(1)} %get-tuple-element.50.refs_0_) | copy-start | bytes 1597444
  14.0 26.9 %collective-permute-start.16 = (bf16[1040,256]{1,0:T(8,128)(2,1)S(1)}, bf16[1040,256]{1,0:T(8,128)(2,1)S(1)}, u32[]{:S(2)}, u32[]{:S(2)}) collective-permute-start(bf16[1040,256]{1,0:T(8,128)(2,1)S(1)} %get-tuple-element.101), channel_id=1, source_target_pairs={{0,4},{4,0},{1,5},{5,1},{2,6},{6,2},{3,7},{7,3},{8,12},{12,8},{9,1... | collective-permute-start | bytes 1597448 | tf_op jit(solution)/shard_map/ppermute | solution.py:200
  15.1 30.3 %collective-permute-start.19 = (bf16[1040,256]{1,0:T(8,128)(2,1)S(1)}, bf16[1040,256]{1,0:T(8,128)(2,1)S(1)}, u32[]{:S(2)}, u32[]{:S(2)}) collective-permute-start(bf16[1040,256]{1,0:T(8,128)(2,1)S(1)} %get-tuple-element.50.refs_0_), channel_id=1, source_target_pairs={{24,16},{16,8},{25,17},{17,9},{26,18},{18,10},{27,19},{19,11},{28,... | collective-permute-start | bytes 1597448 | tf_op jit(solution)/shard_map/ppermute | solution.py:416
  15.8 31.1 %collective-permute-start.17 = (bf16[1040,256]{1,0:T(8,128)(2,1)S(1)}, bf16[1040,256]{1,0:T(8,128)(2,1)S(1)}, u32[]{:S(2)}, u32[]{:S(2)}) collective-permute-start(bf16[1040,256]{1,0:T(8,128)(2,1)S(1)} %get-tuple-element.50.refs_0_), channel_id=1, source_target_pairs={{0,8},{8,16},{1,9},{9,17},{2,10},{10,18},{3,11},{11,19},{4,12},{12... | collective-permute-start | bytes 1597448 | tf_op jit(solution)/shard_map/ppermute | solution.py:415
  41.0 14.2 %collective-permute-start.18 = (bf16[1040,256]{1,0:T(8,128)(2,1)S(1)}, bf16[1040,256]{1,0:T(8,128)(2,1)S(1)}, u32[]{:S(2)}, u32[]{:S(2)}) collective-permute-start(bf16[1040,256]{1,0:T(8,128)(2,1)S(1)} %collective-permute-done.16.refs_1_), channel_id=1, source_target_pairs={{0,8},{8,16},{1,9},{9,17},{2,10},{10,18},{3,11},{11,19},{4,12},{12... | collective-permute-start | bytes 1597448 | tf_op jit(solution)/shard_map/ppermute | solution.py:415
  44.7 5.2 %collective-permute-start.20 = (bf16[1040,256]{1,0:T(8,128)(2,1)S(1)}, bf16[1040,256]{1,0:T(8,128)(2,1)S(1)}, u32[]{:S(2)}, u32[]{:S(2)}) collective-permute-start(bf16[1040,256]{1,0:T(8,128)(2,1)S(1)} %collective-permute-done.16.refs_1_), channel_id=1, source_target_pairs={{24,16},{16,8},{25,17},{17,9},{26,18},{18,10},{27,19},{19,11},{28,... | collective-permute-start | bytes 1597448 | tf_op jit(solution)/shard_map/ppermute | solution.py:416
  45.4 11.7 %collective-permute-start.21 = (bf16[1040,256]{1,0:T(8,128)(2,1)S(1)}, bf16[1040,256]{1,0:T(8,128)(2,1)}, u32[]{:S(2)}, u32[]{:S(2)}) collective-permute-start(bf16[1040,256]{1,0:T(8,128)(2,1)S(1)} %collective-permute-done.19.refs_4_), channel_id=1, source_target_pairs={{16,8},{17,9},{18,10},{19,11},{20,12},{21,13},{22,14},{23,15}} | collective-permute-start | bytes 1597448 | tf_op jit(solution)/shard_map/ppermute | solution.py:418
  46.9 10.2 %collective-permute-start.22 = (bf16[1040,256]{1,0:T(8,128)(2,1)S(1)}, bf16[1040,256]{1,0:T(8,128)(2,1)}, u32[]{:S(2)}, u32[]{:S(2)}) collective-permute-start(bf16[1040,256]{1,0:T(8,128)(2,1)S(1)} %collective-permute-done.17.refs_2_), channel_id=1, source_target_pairs={{8,16},{9,17},{10,18},{11,19},{12,20},{13,21},{14,22},{15,23}} | collective-permute-start | bytes 1597448 | tf_op jit(solution)/shard_map/ppermute | solution.py:417
  49.9 9.2 %collective-permute-start.23 = (bf16[1040,256]{1,0:T(8,128)(2,1)S(1)}, bf16[1040,256]{1,0:T(8,128)(2,1)}, u32[]{:S(2)}, u32[]{:S(2)}) collective-permute-start(bf16[1040,256]{1,0:T(8,128)(2,1)S(1)} %collective-permute-done.20.refs_5_), channel_id=1, source_target_pairs={{16,8},{17,9},{18,10},{19,11},{20,12},{21,13},{22,14},{23,15}} | collective-permute-start | bytes 1597448 | tf_op jit(solution)/shard_map/ppermute | solution.py:418
  55.2 3.9 collective-permute-start.24
  59.0 112.0 %copy-start.56 = (f32[1,256]{1,0:T(1,128)S(1)}, f32[1,256]{1,0:T(1,128)}, u32[]{:S(2)}) copy-start(f32[1,256]{1,0:T(1,128)} %param.31) | copy-start | bytes 3076
  59.0 121.5 %copy-start.53 = (f32[3,512]{1,0:T(4,128)S(1)}, f32[3,512]{1,0:T(4,128)}, u32[]{:S(2)}) copy-start(f32[3,512]{1,0:T(4,128)} %param.22) | copy-start | bytes 18436
  59.0 121.5 %copy-start.54 = (f32[3,512]{1,0:T(4,128)S(1)}, f32[3,512]{1,0:T(4,128)}, u32[]{:S(2)}) copy-start(f32[3,512]{1,0:T(4,128)} %param.21) | copy-start | bytes 18436
  59.0 121.5 %copy-start.37 = (f32[2048]{0:T(1024)S(1)}, f32[2048]{0:T(1024)}, u32[]{:S(2)}) copy-start(f32[2048]{0:T(1024)} %param.17) | copy-start | bytes 24580
  60.0 301.3 %all-gather.7.cloned.1.call-start = ((), (), s32[]{:S(2)}) async-start(), calls=%async_computation.1 | async-start | bytes 3686400 | tf_op jit(solution)/shard_map/all_gather | solution.py:501
  60.0 55.8 %collective-permute-start.7 = (bf16[768,512]{1,0:T(8,128)(2,1)}, bf16[768,512]{1,0:T(8,128)(2,1)S(1)}, u32[]{:S(2)}, u32[]{:S(2)}) collective-permute-start(bf16[768,512]{1,0:T(8,128)(2,1)} %bitcast.b0), channel_id=1, source_target_pairs={{0,8},{24,16},{1,9},{25,17},{2,10},{26,18},{3,11},{27,19},{4,12},{... | collective-permute-start | bytes 2359304 | tf_op jit(solution)/shard_map/ppermute | solution.py:405
  115.8 84.6 %copy-start.4 = (bf16[768,512]{1,0:T(8,128)(2,1)}, bf16[768,512]{1,0:T(8,128)(2,1)S(1)}, u32[]{:S(2)}) copy-start(bf16[768,512]{1,0:T(8,128)(2,1)S(1)} %collective-permute-done.7.b0) | copy-start | bytes 2359300
  115.8 18.6 %collective-permute-start.11 = (bf16[768,512]{1,0:T(8,128)(2,1)S(1)}, bf16[768,512]{1,0:T(8,128)(2,1)S(1)}, u32[]{:S(2)}, u32[]{:S(2)}) collective-permute-start(bf16[768,512]{1,0:T(8,128)(2,1)S(1)} %collective-permute-done.7.b0), channel_id=1, source_target_pairs={{0,4},{4,0},{1,5},{5,1},{2,6},{6,2},{3,7},{7,3},{8,12},{12,8},{9,1... | collective-permute-start | bytes 2359304 | tf_op jit(solution)/shard_map/ppermute | solution.py:200
  117.1 25.8 %collective-permute-start.3 = (bf16[768,512]{1,0:T(8,128)(2,1)}, bf16[768,512]{1,0:T(8,128)(2,1)}, u32[]{:S(2)}, u32[]{:S(2)}) collective-permute-start(bf16[768,512]{1,0:T(8,128)(2,1)} %bitcast.b0), channel_id=1, source_target_pairs={{0,4},{4,0},{1,5},{5,1},{2,6},{6,2},{3,7},{7,3},{8,12},{12,8},{9,1... | collective-permute-start | bytes 2359304 | tf_op jit(solution)/shard_map/ppermute | solution.py:200
  117.8 26.4 %collective-permute-start = (bf16[768,512]{1,0:T(8,128)(2,1)}, bf16[768,512]{1,0:T(8,128)(2,1)}, u32[]{:S(2)}, u32[]{:S(2)}) collective-permute-start(bf16[768,512]{1,0:T(8,128)(2,1)} %bitcast.b0), channel_id=1, source_target_pairs={{0,2},{2,0},{1,3},{3,1},{4,6},{6,4},{5,7},{7,5},{8,10},{10,8},{9,1... | collective-permute-start | bytes 2359304 | tf_op jit(solution)/shard_map/ppermute | solution.py:200
  134.4 20.9 %collective-permute-start.12 = (bf16[768,512]{1,0:T(8,128)(2,1)S(1)}, bf16[768,512]{1,0:T(8,128)(2,1)S(1)}, u32[]{:S(2)}, u32[]{:S(2)}) collective-permute-start(bf16[768,512]{1,0:T(8,128)(2,1)S(1)} %collective-permute-done.11.b0), channel_id=1, source_target_pairs={{0,2},{2,0},{1,3},{3,1},{4,6},{6,4},{5,7},{7,5},{8,10},{10,8},{9,1... | collective-permute-start | bytes 2359304 | tf_op jit(solution)/shard_map/ppermute | solution.py:200
  135.7 35.4 %collective-permute-start.8 = (bf16[768,512]{1,0:T(8,128)(2,1)S(1)}, bf16[768,512]{1,0:T(8,128)(2,1)}, u32[]{:S(2)}, u32[]{:S(2)}) collective-permute-start(bf16[768,512]{1,0:T(8,128)(2,1)S(1)} %collective-permute-done.7.b0), channel_id=1, source_target_pairs={{0,2},{2,0},{1,3},{3,1},{4,6},{6,4},{5,7},{7,5},{8,10},{10,8},{9,1... | collective-permute-start | bytes 2359304 | tf_op jit(solution)/shard_map/ppermute | solution.py:200
  142.9 36.5 %collective-permute-start.4 = (bf16[768,512]{1,0:T(8,128)(2,1)}, bf16[768,512]{1,0:T(8,128)(2,1)}, u32[]{:S(2)}, u32[]{:S(2)}) collective-permute-start(bf16[768,512]{1,0:T(8,128)(2,1)} %collective-permute-done.3.b0), channel_id=1, source_target_pairs={{0,2},{2,0},{1,3},{3,1},{4,6},{6,4},{5,7},{7,5},{8,10},{10,8},{9,1... | collective-permute-start | bytes 2359304 | tf_op jit(solution)/shard_map/ppermute | solution.py:200
  144.2 35.3 %collective-permute-start.9 = (bf16[768,512]{1,0:T(8,128)(2,1)S(1)}, bf16[768,512]{1,0:T(8,128)(2,1)}, u32[]{:S(2)}, u32[]{:S(2)}) collective-permute-start(bf16[768,512]{1,0:T(8,128)(2,1)S(1)} %collective-permute-done.7.b0), channel_id=1, source_target_pairs={{0,1},{1,0},{2,3},{3,2},{4,5},{5,4},{6,7},{7,6},{8,9},{9,8},{10,11... | collective-permute-start | bytes 2359304 | tf_op jit(solution)/shard_map/ppermute | solution.py:200
  144.2 35.8 %collective-permute-start.13 = (bf16[768,512]{1,0:T(8,128)(2,1)S(1)}, bf16[768,512]{1,0:T(8,128)(2,1)}, u32[]{:S(2)}, u32[]{:S(2)}) collective-permute-start(bf16[768,512]{1,0:T(8,128)(2,1)S(1)} %collective-permute-done.11.b0), channel_id=1, source_target_pairs={{0,1},{1,0},{2,3},{3,2},{4,5},{5,4},{6,7},{7,6},{8,9},{9,8},{10,11... | collective-permute-start | bytes 2359304 | tf_op jit(solution)/shard_map/ppermute | solution.py:200
  155.3 24.7 %collective-permute-start.14 = (bf16[768,512]{1,0:T(8,128)(2,1)S(1)}, bf16[768,512]{1,0:T(8,128)(2,1)}, u32[]{:S(2)}, u32[]{:S(2)}) collective-permute-start(bf16[768,512]{1,0:T(8,128)(2,1)S(1)} %collective-permute-done.12.b1), channel_id=1, source_target_pairs={{0,1},{1,0},{2,3},{3,2},{4,5},{5,4},{6,7},{7,6},{8,9},{9,8},{10,11... | collective-permute-start | bytes 2359304 | tf_op jit(solution)/shard_map/ppermute | solution.py:200
  171.0 29.3 %collective-permute-start.10 = (bf16[768,512]{1,0:T(8,128)(2,1)}, bf16[768,512]{1,0:T(8,128)(2,1)S(1)}, u32[]{:S(2)}, u32[]{:S(2)}) collective-permute-start(bf16[768,512]{1,0:T(8,128)(2,1)} %collective-permute-done.8.b1), channel_id=1, source_target_pairs={{0,1},{1,0},{2,3},{3,2},{4,5},{5,4},{6,7},{7,6},{8,9},{9,8},{10,11... | collective-permute-start | bytes 2359304 | tf_op jit(solution)/shard_map/ppermute | solution.py:200
  179.5 33.2 %collective-permute-start.1 = (bf16[768,512]{1,0:T(8,128)(2,1)}, bf16[768,512]{1,0:T(8,128)(2,1)S(1)}, u32[]{:S(2)}, u32[]{:S(2)}) collective-permute-start(bf16[768,512]{1,0:T(8,128)(2,1)} %bitcast.b0), channel_id=1, source_target_pairs={{0,1},{1,0},{2,3},{3,2},{4,5},{5,4},{6,7},{7,6},{8,9},{9,8},{10,11... | collective-permute-start | bytes 2359304 | tf_op jit(solution)/shard_map/ppermute | solution.py:200
  179.5 33.2 %collective-permute-start.5 = (bf16[768,512]{1,0:T(8,128)(2,1)}, bf16[768,512]{1,0:T(8,128)(2,1)S(1)}, u32[]{:S(2)}, u32[]{:S(2)}) collective-permute-start(bf16[768,512]{1,0:T(8,128)(2,1)} %collective-permute-done.3.b0), channel_id=1, source_target_pairs={{0,1},{1,0},{2,3},{3,2},{4,5},{5,4},{6,7},{7,6},{8,9},{9,8},{10,11... | collective-permute-start | bytes 2359304 | tf_op jit(solution)/shard_map/ppermute | solution.py:200
  180.0 32.7 %collective-permute-start.2 = (bf16[768,512]{1,0:T(8,128)(2,1)}, bf16[768,512]{1,0:T(8,128)(2,1)S(1)}, u32[]{:S(2)}, u32[]{:S(2)}) collective-permute-start(bf16[768,512]{1,0:T(8,128)(2,1)} %collective-permute-done.b1), channel_id=1, source_target_pairs={{0,1},{1,0},{2,3},{3,2},{4,5},{5,4},{6,7},{7,6},{8,9},{9,8},{10,11... | collective-permute-start | bytes 2359304 | tf_op jit(solution)/shard_map/ppermute | solution.py:200
  180.1 32.6 %collective-permute-start.6 = (bf16[768,512]{1,0:T(8,128)(2,1)}, bf16[768,512]{1,0:T(8,128)(2,1)S(1)}, u32[]{:S(2)}, u32[]{:S(2)}) collective-permute-start(bf16[768,512]{1,0:T(8,128)(2,1)} %collective-permute-done.4.b1), channel_id=1, source_target_pairs={{0,1},{1,0},{2,3},{3,2},{4,5},{5,4},{6,7},{7,6},{8,9},{9,8},{10,11... | collective-permute-start | bytes 2359304 | tf_op jit(solution)/shard_map/ppermute | solution.py:200
  200.4 38.0 %collective-permute-start.34 = (bf16[2,2,768,256]{3,2,1,0:T(8,128)(2,1)}, bf16[2,2,768,256]{3,2,1,0:T(8,128)(2,1)}, u32[]{:S(2)}, u32[]{:S(2)}) collective-permute-start(bf16[2,2,768,256]{3,2,1,0:T(8,128)(2,1)} %get-tuple-element.87), channel_id=1, source_target_pairs={{0,1},{1,0},{2,3},{3,2},{4,5},{5,4},{6,7},{7,6},{8,9},{9,8},{10,11... | collective-permute-start | bytes 4718600 | tf_op jit(solution)/shard_map/ppermute | solution.py:200
  223.9 13.4 %collective-permute-start.43 = (bf16[720,256]{1,0:T(8,128)(2,1)S(1)}, bf16[720,256]{1,0:T(8,128)(2,1)S(1)}, u32[]{:S(2)}, u32[]{:S(2)}) collective-permute-start(bf16[720,256]{1,0:T(8,128)(2,1)S(1)} %broadcast_select_fusion.7), channel_id=1, source_target_pairs={{0,4},{4,0},{1,5},{5,1},{2,6},{6,2},{3,7},{7,3},{8,12},{12,8},{9,1... | collective-permute-start | bytes 1105928 | tf_op jit(solution)/shard_map/ppermute | solution.py:200
  225.2 17.0 %collective-permute-start.32 = (bf16[2,2,768,256]{3,2,1,0:T(8,128)(2,1)}, bf16[2,2,768,256]{3,2,1,0:T(8,128)(2,1)}, u32[]{:S(2)}, u32[]{:S(2)}) collective-permute-start(bf16[2,2,768,256]{3,2,1,0:T(8,128)(2,1)} %get-tuple-element.85), channel_id=1, source_target_pairs={{0,1},{1,0},{2,3},{3,2},{4,5},{5,4},{6,7},{7,6},{8,9},{9,8},{10,11... | collective-permute-start | bytes 4718600 | tf_op jit(solution)/shard_map/ppermute | solution.py:200
  236.8 11.7 %collective-permute-start.25 = (bf16[2,2,768,256]{3,2,1,0:T(8,128)(2,1)}, bf16[2,2,768,256]{3,2,1,0:T(8,128)(2,1)}, u32[]{:S(2)}, u32[]{:S(2)}) collective-permute-start(bf16[2,2,768,256]{3,2,1,0:T(8,128)(2,1)} %get-tuple-element.81), channel_id=1, source_target_pairs={{0,1},{1,0},{2,3},{3,2},{4,5},{5,4},{6,7},{7,6},{8,9},{9,8},{10,11... | collective-permute-start | bytes 4718600 | tf_op jit(solution)/shard_map/ppermute | solution.py:200
  237.1 7.9 %collective-permute-start.27 = (bf16[2,2,768,256]{3,2,1,0:T(8,128)(2,1)}, bf16[2,2,768,256]{3,2,1,0:T(8,128)(2,1)}, u32[]{:S(2)}, u32[]{:S(2)}) collective-permute-start(bf16[2,2,768,256]{3,2,1,0:T(8,128)(2,1)} %get-tuple-element.83), channel_id=1, source_target_pairs={{0,1},{1,0},{2,3},{3,2},{4,5},{5,4},{6,7},{7,6},{8,9},{9,8},{10,11... | collective-permute-start | bytes 4718600 | tf_op jit(solution)/shard_map/ppermute | solution.py:200
  240.3 31.8 %collective-permute-start.37 = (bf16[2,768,256]{2,1,0:T(8,128)(2,1)S(1)}, bf16[2,768,256]{2,1,0:T(8,128)(2,1)S(1)}, u32[]{:S(2)}, u32[]{:S(2)}) collective-permute-start(bf16[2,768,256]{2,1,0:T(8,128)(2,1)S(1)} %slice_bitcast_fusion.8), channel_id=1, source_target_pairs={{0,4},{4,0},{1,5},{5,1},{2,6},{6,2},{3,7},{7,3},{8,12},{12,8},{9,1... | collective-permute-start | bytes 2359304 | tf_op jit(solution)/shard_map/ppermute | solution.py:200
  241.0 12.0 %collective-permute-start.35 = (bf16[768,256]{1,0:T(8,128)(2,1)S(1)}, bf16[768,256]{1,0:T(8,128)(2,1)S(1)}, u32[]{:S(2)}, u32[]{:S(2)}) collective-permute-start(bf16[768,256]{1,0:T(8,128)(2,1)S(1)} %slice_bitcast_fusion.16), channel_id=1, source_target_pairs={{0,2},{2,0},{1,3},{3,1},{4,6},{6,4},{5,7},{7,5},{8,10},{10,8},{9,1... | collective-permute-start | bytes 1179656 | tf_op jit(solution)/shard_map/ppermute | solution.py:200
  244.1 35.1 %collective-permute-start.33 = (bf16[768,256]{1,0:T(8,128)(2,1)S(1)}, bf16[768,256]{1,0:T(8,128)(2,1)S(1)}, u32[]{:S(2)}, u32[]{:S(2)}) collective-permute-start(bf16[768,256]{1,0:T(8,128)(2,1)S(1)} %fusion.24), channel_id=1, source_target_pairs={{0,2},{2,0},{1,3},{3,1},{4,6},{6,4},{5,7},{7,5},{8,10},{10,8},{9,1... | collective-permute-start | bytes 1179656 | tf_op jit(solution)/shard_map/ppermute | solution.py:200
  246.9 30.7 %collective-permute-start.30 = (bf16[2,768,256]{2,1,0:T(8,128)(2,1)S(1)}, bf16[2,768,256]{2,1,0:T(8,128)(2,1)S(1)}, u32[]{:S(2)}, u32[]{:S(2)}) collective-permute-start(bf16[2,768,256]{2,1,0:T(8,128)(2,1)S(1)} %slice_bitcast_fusion.12), channel_id=1, source_target_pairs={{0,4},{4,0},{1,5},{5,1},{2,6},{6,2},{3,7},{7,3},{8,12},{12,8},{9,1... | collective-permute-start | bytes 2359304 | tf_op jit(solution)/shard_map/ppermute | solution.py:200
  248.4 21.4 %collective-permute-start.28 = (bf16[768,256]{1,0:T(8,128)(2,1)S(1)}, bf16[768,256]{1,0:T(8,128)(2,1)S(1)}, u32[]{:S(2)}, u32[]{:S(2)}) collective-permute-start(bf16[768,256]{1,0:T(8,128)(2,1)S(1)} %slice_bitcast_fusion.17), channel_id=1, source_target_pairs={{0,2},{2,0},{1,3},{3,1},{4,6},{6,4},{5,7},{7,5},{8,10},{10,8},{9,1... | collective-permute-start | bytes 1179656 | tf_op jit(solution)/shard_map/ppermute | solution.py:200
  253.0 39.3 %collective-permute-start.26 = (bf16[768,256]{1,0:T(8,128)(2,1)}, bf16[768,256]{1,0:T(8,128)(2,1)S(1)}, u32[]{:S(2)}, u32[]{:S(2)}) collective-permute-start(bf16[768,256]{1,0:T(8,128)(2,1)} %fusion.22), channel_id=1, source_target_pairs={{0,2},{2,0},{1,3},{3,1},{4,6},{6,4},{5,7},{7,5},{8,10},{10,8},{9,1... | collective-permute-start | bytes 1179656 | tf_op jit(solution)/shard_map/ppermute | solution.py:200
  269.9 16.2 %collective-permute-start.36 = (bf16[768,256]{1,0:T(8,128)(2,1)S(1)}, bf16[768,256]{1,0:T(8,128)(2,1)S(1)}, u32[]{:S(2)}, u32[]{:S(2)}) collective-permute-start(bf16[768,256]{1,0:T(8,128)(2,1)S(1)} %fusion.14), channel_id=1, source_target_pairs={{0,4},{4,0},{1,5},{5,1},{2,6},{6,2},{3,7},{7,3},{8,12},{12,8},{9,1... | collective-permute-start | bytes 1179656 | tf_op jit(solution)/shard_map/ppermute | solution.py:200
  272.1 21.9 %collective-permute-start.29 = (bf16[768,256]{1,0:T(8,128)(2,1)}, bf16[768,256]{1,0:T(8,128)(2,1)}, u32[]{:S(2)}, u32[]{:S(2)}) collective-permute-start(bf16[768,256]{1,0:T(8,128)(2,1)} %fusion.19), channel_id=1, source_target_pairs={{0,4},{4,0},{1,5},{5,1},{2,6},{6,2},{3,7},{7,3},{8,12},{12,8},{9,1... | collective-permute-start | bytes 1179656 | tf_op jit(solution)/shard_map/ppermute | solution.py:200
  277.6 10.0 %collective-permute-start.38 = (bf16[768,256]{1,0:T(8,128)(2,1)S(1)}, bf16[768,256]{1,0:T(8,128)(2,1)S(1)}, u32[]{:S(2)}, u32[]{:S(2)}) collective-permute-start(bf16[768,256]{1,0:T(8,128)(2,1)S(1)} %fusion.25), channel_id=1, source_target_pairs={{0,2},{2,0},{1,3},{3,1},{4,6},{6,4},{5,7},{7,5},{8,10},{10,8},{9,1... | collective-permute-start | bytes 1179656 | tf_op jit(solution)/shard_map/ppermute | solution.py:200
  288.8 24.0 %collective-permute-start.39 = (bf16[768,512]{1,0:T(8,128)(2,1)}, bf16[768,512]{1,0:T(8,128)(2,1)}, u32[]{:S(2)}, u32[]{:S(2)}) collective-permute-start(bf16[768,512]{1,0:T(8,128)(2,1)} %fusion.4), channel_id=1, source_target_pairs={{8,0},{16,24},{9,1},{17,25},{10,2},{18,26},{11,3},{19,27},{12,4},{... | collective-permute-start | bytes 2359304 | tf_op jit(solution)/shard_map/ppermute | solution.py:496
  290.8 9.5 %collective-permute-start.31 = (bf16[768,256]{1,0:T(8,128)(2,1)}, bf16[768,256]{1,0:T(8,128)(2,1)}, u32[]{:S(2)}, u32[]{:S(2)}) collective-permute-start(bf16[768,256]{1,0:T(8,128)(2,1)} %fusion.23), channel_id=1, source_target_pairs={{0,2},{2,0},{1,3},{3,1},{4,6},{6,4},{5,7},{7,5},{8,10},{10,8},{9,1... | collective-permute-start | bytes 1179656 | tf_op jit(solution)/shard_map/ppermute | solution.py:200
  314.4 19.3 %collective-permute-start.46 = (bf16[768,512]{1,0:T(8,128)(2,1)S(1)}, bf16[768,512]{1,0:T(8,128)(2,1)S(1)}, u32[]{:S(2)}, u32[]{:S(2)}) collective-permute-start(bf16[768,512]{1,0:T(8,128)(2,1)S(1)} %fusion.6.b0), channel_id=1, source_target_pairs={{0,4},{4,0},{1,5},{5,1},{2,6},{6,2},{3,7},{7,3},{8,12},{12,8},{9,1... | collective-permute-start | bytes 2359304 | tf_op jit(solution)/shard_map/ppermute | solution.py:200
  316.0 19.3 %collective-permute-start.40 = (bf16[768,512]{1,0:T(8,128)(2,1)S(1)}, bf16[768,512]{1,0:T(8,128)(2,1)S(1)}, u32[]{:S(2)}, u32[]{:S(2)}) collective-permute-start(bf16[768,512]{1,0:T(8,128)(2,1)S(1)} %fusion.6.b0), channel_id=1, source_target_pairs={{0,2},{2,0},{1,3},{3,1},{4,6},{6,4},{5,7},{7,5},{8,10},{10,8},{9,1... | collective-permute-start | bytes 2359304 | tf_op jit(solution)/shard_map/ppermute | solution.py:200
  333.7 10.0 %collective-permute-start.47 = (bf16[768,256]{1,0:T(8,128)(2,1)S(1)}, bf16[768,256]{1,0:T(8,128)(2,1)S(1)}, u32[]{:S(2)}, u32[]{:S(2)}) collective-permute-start(bf16[768,256]{1,0:T(8,128)(2,1)S(1)} %slice.322), channel_id=1, source_target_pairs={{0,2},{2,0},{1,3},{3,1},{4,6},{6,4},{5,7},{7,5},{8,10},{10,8},{9,1... | collective-permute-start | bytes 1179656 | tf_op jit(solution)/shard_map/ppermute | solution.py:200
  335.3 9.8 %collective-permute-start.48 = (bf16[768,256]{1,0:T(8,128)(2,1)S(1)}, bf16[768,256]{1,0:T(8,128)(2,1)S(1)}, u32[]{:S(2)}, u32[]{:S(2)}) collective-permute-start(bf16[768,256]{1,0:T(8,128)(2,1)S(1)} %slice.323), channel_id=1, source_target_pairs={{0,4},{4,0},{1,5},{5,1},{2,6},{6,2},{3,7},{7,3},{8,12},{12,8},{9,1... | collective-permute-start | bytes 1179656 | tf_op jit(solution)/shard_map/ppermute | solution.py:200
  336.7 9.7 %collective-permute-start.49 = (bf16[768,512]{1,0:T(8,128)(2,1)S(1)}, bf16[768,512]{1,0:T(8,128)(2,1)}, u32[]{:S(2)}, u32[]{:S(2)}) collective-permute-start(bf16[768,512]{1,0:T(8,128)(2,1)S(1)} %collective-permute-done.46.b0), channel_id=1, source_target_pairs={{0,1},{1,0},{2,3},{3,2},{4,5},{5,4},{6,7},{7,6},{8,9},{9,8},{10,11... | collective-permute-start | bytes 2359304 | tf_op jit(solution)/shard_map/ppermute | solution.py:200
  345.1 2.5 collective-permute-start.50
  345.7 22.4 %collective-permute-start.41 = (bf16[768,512]{1,0:T(8,128)(2,1)S(1)}, bf16[768,512]{1,0:T(8,128)(2,1)}, u32[]{:S(2)}, u32[]{:S(2)}) collective-permute-start(bf16[768,512]{1,0:T(8,128)(2,1)S(1)} %fusion.6.b0), channel_id=1, source_target_pairs={{0,1},{1,0},{2,3},{3,2},{4,5},{5,4},{6,7},{7,6},{8,9},{9,8},{10,11... | collective-permute-start | bytes 2359304 | tf_op jit(solution)/shard_map/ppermute | solution.py:200
  346.2 21.9 %collective-permute-start.42 = (bf16[768,512]{1,0:T(8,128)(2,1)S(1)}, bf16[768,512]{1,0:T(8,128)(2,1)}, u32[]{:S(2)}, u32[]{:S(2)}) collective-permute-start(bf16[768,512]{1,0:T(8,128)(2,1)S(1)} %collective-permute-done.40.b1), channel_id=1, source_target_pairs={{0,1},{1,0},{2,3},{3,2},{4,5},{5,4},{6,7},{7,6},{8,9},{9,8},{10,11... | collective-permute-start | bytes 2359304 | tf_op jit(solution)/shard_map/ppermute | solution.py:200
  367.9 14.0 %collective-permute-start.51 = (bf16[2,2,768,256]{3,2,1,0:T(8,128)(2,1)S(1)}, bf16[2,2,768,256]{3,2,1,0:T(8,128)(2,1)S(1)}, u32[]{:S(2)}, u32[]{:S(2)}) collective-permute-start(bf16[2,2,768,256]{3,2,1,0:T(8,128)(2,1)S(1)} %get-tuple-element.94), channel_id=1, source_target_pairs={{0,1},{1,0},{2,3},{3,2},{4,5},{5,4},{6,7},{7,6},{8,9},{9,8},{10,11... | collective-permute-start | bytes 4718600 | tf_op jit(solution)/shard_map/ppermute | solution.py:200
  381.6 3.5 collective-permute-start.44
  382.5 20.5 %collective-permute-start.54 = (bf16[2,768,256]{2,1,0:T(8,128)(2,1)S(1)}, bf16[2,768,256]{2,1,0:T(8,128)(2,1)S(1)}, u32[]{:S(2)}, u32[]{:S(2)}) collective-permute-start(bf16[2,768,256]{2,1,0:T(8,128)(2,1)S(1)} %slice_bitcast_fusion.4), channel_id=1, source_target_pairs={{0,4},{4,0},{1,5},{5,1},{2,6},{6,2},{3,7},{7,3},{8,12},{12,8},{9,1... | collective-permute-start | bytes 2359304 | tf_op jit(solution)/shard_map/ppermute | solution.py:200
  383.6 12.1 %collective-permute-start.52 = (bf16[768,256]{1,0:T(8,128)(2,1)S(1)}, bf16[768,256]{1,0:T(8,128)(2,1)S(1)}, u32[]{:S(2)}, u32[]{:S(2)}) collective-permute-start(bf16[768,256]{1,0:T(8,128)(2,1)S(1)} %slice_bitcast_fusion.15), channel_id=1, source_target_pairs={{0,2},{2,0},{1,3},{3,1},{4,6},{6,4},{5,7},{7,5},{8,10},{10,8},{9,1... | collective-permute-start | bytes 1179656 | tf_op jit(solution)/shard_map/ppermute | solution.py:200
  385.5 18.5 %collective-permute-start.45 = (bf16[768,256]{1,0:T(8,128)(2,1)S(1)}, bf16[768,256]{1,0:T(8,128)(2,1)S(1)}, u32[]{:S(2)}, u32[]{:S(2)}) collective-permute-start(bf16[768,256]{1,0:T(8,128)(2,1)S(1)} %fusion.26), channel_id=1, source_target_pairs={{0,2},{2,0},{1,3},{3,1},{4,6},{6,4},{5,7},{7,5},{8,10},{10,8},{9,1... | collective-permute-start | bytes 1179656 | tf_op jit(solution)/shard_map/ppermute | solution.py:200
  395.8 14.9 %collective-permute-start.53 = (bf16[768,256]{1,0:T(8,128)(2,1)S(1)}, bf16[768,256]{1,0:T(8,128)(2,1)S(1)}, u32[]{:S(2)}, u32[]{:S(2)}) collective-permute-start(bf16[768,256]{1,0:T(8,128)(2,1)S(1)} %fusion.9), channel_id=1, source_target_pairs={{0,4},{4,0},{1,5},{5,1},{2,6},{6,2},{3,7},{7,3},{8,12},{12,8},{9,1... | collective-permute-start | bytes 1179656 | tf_op jit(solution)/shard_map/ppermute | solution.py:200
  403.2 9.8 %collective-permute-start.55 = (bf16[768,256]{1,0:T(8,128)(2,1)S(1)}, bf16[768,256]{1,0:T(8,128)(2,1)S(1)}, u32[]{:S(2)}, u32[]{:S(2)}) collective-permute-start(bf16[768,256]{1,0:T(8,128)(2,1)S(1)} %fusion.27), channel_id=1, source_target_pairs={{0,2},{2,0},{1,3},{3,1},{4,6},{6,4},{5,7},{7,5},{8,10},{10,8},{9,1... | collective-permute-start | bytes 1179656 | tf_op jit(solution)/shard_map/ppermute | solution.py:200
  (51 other events, 316.5 us)
Sparse Core Ops, SparseCore 0:
  60.1 135.7 all-gather.4
  238.5 59.4 all-gather.6
